TPU v7x, 256 devices: a whole 4x4x8 slice. The times are simulated.
256 devices in a mesh: sp: 32 (over z, x), tp: 8 (over y, core).
Axes of the slice: x: 4, y: 4, z: 8, core: 2. Of those that a mesh axis runs over, the one named last changes fastest.
Arguments:
- resid: bfloat16 [12288, 2048], P(('sp', 'tp')), may hold values from -6 to 6
- queries: bfloat16 [12288, 1024], P('sp', 'tp'), may hold values from -6 to 6
- keys: bfloat16 [12288, 1024], P('sp', 'tp'), may hold values from -6 to 6
- values: bfloat16 [12288, 1024], P('sp', 'tp'), may hold values from -6 to 6
- decay_input_part: bfloat16 [12288, 1024], P('sp', 'tp'), may hold values from -4 to 4
- decay_channel_offset: float32 [1024], P('tp'), may hold values from -16 to -2
- decay_head_extra: float32 [12288, 16], P('sp', 'tp'), may hold values from 0 to 0.7
- correction_rate_input: bfloat16 [12288, 1024], P('sp', 'tp'), may hold values from -6 to 6
- correction_rate_offset: float32 [1024], P('tp'), may hold values from -0.4 to 1
- head_norm_gain: float32 [1024], P('tp'), may hold values from 0.1 to 1.9
- mixer_output_weight: bfloat16 [1024, 2048], replicated, may hold values from -0.1875 to 0.1875
- feedforward_norm_gain: float32 [2048], replicated, may hold values from 0.1 to 1.9
- gate_weight: bfloat16 [2048, 5632], P('sp', 'tp'), may hold values from -0.125 to 0.125
- up_weight: bfloat16 [2048, 5632], P('sp', 'tp'), may hold values from -0.125 to 0.125
- down_weight: bfloat16 [5632, 2048], P('tp', 'sp'), may hold values from -0.078125 to 0.078125
Outputs:
- result: bfloat16 [12288, 2048], P(('sp', 'tp'))
All inputs are finite; a program needn't handle non-finite values.
Results may differ from a plain program's by a relative error of at most 0.014.
Values may be sent and summed in bfloat16 or wider, within the bound.
A program may use at most 64 MiB of HBM per device.

v0:
```python
import jax
import jax.numpy as jnp
from jax import lax
from jax.sharding import Mesh
from jax.sharding import PartitionSpec as P

HEAD = 64
BLK = 16
SP = ("sp_0", "sp_1")
SP_TP = ("sp_0", "sp_1", "tp")


def nothing_yet(array, identity):
    return jax.tree.map(
        lambda a, e: jnp.broadcast_to(jnp.asarray(e, a.dtype), a.shape), array, identity
    )


def gathered_once(array, axis):
    leaves = jax.tree.leaves(array)
    sequence = sorted(range(len(leaves)), key=lambda k: -leaves[k].size)
    width = (1, *leaves[sequence[0]].shape)[-1]
    lines = [
        jnp.pad(leaves[k].reshape(-1), (0, -leaves[k].size % width)).reshape(-1, width)
        for k in sequence
    ]
    both, at, found = (lax.all_gather(jnp.concatenate(lines), axis), 0, {})
    for k, line in zip(sequence, lines):
        piece = both[:, at : at + len(line)].reshape(len(both), -1)
        found[k] = piece[:, : leaves[k].size].reshape(-1, *leaves[k].shape)
        at += len(line)
    numbers = iter(range(len(leaves)))
    return jax.tree.map(lambda _: found[next(numbers)], array)


def entering(array, axes, combine, identity):
    before = start = nothing_yet(array, identity)
    total = array
    for axis in reversed(axes):
        count, index = (lax.axis_size(axis), lax.axis_index(axis))
        pieces = gathered_once(
            jax.tree.map(
                lambda part, kind: part.astype(kind),
                total,
                jax.tree.map(lambda a: jnp.bfloat16 if a.dtype == jnp.float32 else a.dtype, array),
            ),
            axis,
        )
        inside, total = (start, start)
        for k in range(count):
            passed = k < index
            total = combine(
                total, jax.tree.map(lambda part, own: part[k].astype(own.dtype), pieces, array)
            )
            inside = jax.tree.map(lambda new, old: jnp.where(passed, new, old), total, inside)
        before = combine(inside, before)
    return before


def joined_along(pieces, dim):
    pieces = jnp.moveaxis(pieces, 0, dim)
    lengths = pieces.shape
    return pieces.reshape(*lengths[:dim], lengths[dim] * lengths[dim + 1], *lengths[dim + 2 :])


def from_everyone(array, axis):
    copies = jnp.broadcast_to(array, (lax.axis_size(axis), *array.shape))
    return lax.all_to_all(copies, axis, split_axis=0, concat_axis=0, tiled=True)


def gathered_copies(array, axis, dim):
    return joined_along(from_everyone(array, axis), dim)


def sent_together(arrays, axis, dim, along):
    both = jnp.concatenate(arrays, axis=along)
    whole, at, outs = (lax.all_gather(both, axis, axis=dim, tiled=True), 0, [])
    for a in arrays:
        outs.append(lax.slice_in_dim(whole, at, at + a.shape[along], axis=along))
        at += a.shape[along]
    return tuple(outs)


def whole_of(array, axes, dim):
    whole = array
    for number in range(len(axes) - 1, -1, -1):
        whole = lax.all_gather(whole, axes[number], axis=dim, tiled=True)
    return whole


def cut_along(array, dim, count):
    before, after = (array.shape[:dim], array.shape[dim + 1 :])
    return jnp.moveaxis(array.reshape(*before, count, -1, *after), dim, 0)


def sent_and_summed(array, axis, dim):
    count = lax.axis_size(axis)
    pieces = lax.all_to_all(cut_along(array, dim, count), axis, 0, 0, tiled=True)
    return jnp.sum(pieces.astype(jnp.float32), axis=0)


def matmul(left, right):
    return jnp.einsum("...ij,...jk->...ik", left, right, precision=lax.Precision.HIGHEST)


def combine(earlier, later):
    return (matmul(earlier[0], later[0]), matmul(earlier[1], later[0]) + later[1])


def block_step(carry, inputs):
    state, trans = carry
    query_t, decay_t, key_t, value_t, unit_t, lrate_t = inputs
    lifted = -unit_t
    state_dir = jnp.einsum("bhvk,bhk->bhv", state, lifted, precision=lax.Precision.HIGHEST)
    trans_dir = jnp.einsum("bhjk,bhk->bhj", trans, lifted, precision=lax.Precision.HIGHEST)
    scaled = unit_t * lrate_t
    state = (
        state * decay_t[:, :, None, :]
        + state_dir[..., None] * scaled[:, :, None, :]
        + value_t[..., None] * key_t[:, :, None, :]
    )
    trans = trans * decay_t[:, :, None, :] + trans_dir[..., None] * scaled[:, :, None, :]
    own_read = jnp.einsum("bhvk,bhk->bhv", state, query_t, precision=lax.Precision.HIGHEST)
    trans_read = jnp.einsum("bhjk,bhk->bhj", trans, query_t, precision=lax.Precision.HIGHEST)
    return ((state, trans), (own_read, trans_read))


def per_device(
    resid,
    queries,
    keys,
    values,
    decay_input_part,
    decay_channel_offset,
    decay_head_extra,
    correction_rate_input,
    correction_rate_offset,
    head_norm_gain,
    mixer_output_weight,
    feedforward_norm_gain,
    gate_weight,
    up_weight,
    down_weight,
):
    tok_rows = queries.shape[0]
    local_heads = queries.shape[1] // HEAD
    blocks = tok_rows // BLK

    def head_count(arr):
        return arr.astype(jnp.float32).reshape(tok_rows, local_heads, HEAD)

    def to_steps(arr):
        return jnp.moveaxis(arr.reshape(blocks, BLK, local_heads, HEAD), 1, 0)

    correction_rate = jnp.exp(
        -jax.nn.softplus(-(decay_channel_offset + decay_input_part.astype(jnp.float32))) - 0.5
    )
    decay_factor = jnp.exp(-head_count(correction_rate) - decay_head_extra[:, :, None])
    key_f = head_count(keys)
    unit_keys = key_f * lax.rsqrt(jnp.sum(key_f * key_f, axis=-1, keepdims=True) + 1e-06)
    lrate = head_count(
        jax.nn.sigmoid(correction_rate_offset + correction_rate_input.astype(jnp.float32))
    )
    identity = jnp.broadcast_to(jnp.eye(HEAD, dtype=jnp.float32), (local_heads, HEAD, HEAD))
    zeros = jnp.zeros((local_heads, HEAD, HEAD), jnp.float32)
    start = (
        jnp.zeros((blocks, local_heads, HEAD, HEAD), jnp.float32),
        jnp.broadcast_to(identity, (blocks, local_heads, HEAD, HEAD)),
    )
    step_inputs = tuple(
        (
            to_steps(arr)
            for arr in (
                head_count(queries),
                decay_factor,
                key_f,
                head_count(values),
                unit_keys,
                lrate,
            )
        )
    )
    (end_state, end_trans), (own_read, trans_read) = lax.scan(block_step, start, step_inputs)
    inclusive = lax.associative_scan(combine, (end_trans, end_state), axis=0)
    device_total = (inclusive[0][-1], inclusive[1][-1])
    prefix_trans = jnp.concatenate([identity[None], inclusive[0][:-1]], axis=0)
    prefix_state = jnp.concatenate([zeros[None], inclusive[1][:-1]], axis=0)
    _, incoming = entering(device_total, SP, combine, (identity, zeros))
    block_start = (
        jnp.einsum("hvk,bhkj->bhvj", incoming, prefix_trans, precision=lax.Precision.HIGHEST)
        + prefix_state
    )
    reads = (
        jnp.einsum("bhvk,tbhk->tbhv", block_start, trans_read, precision=lax.Precision.HIGHEST)
        + own_read
    )
    mixer_out = jnp.moveaxis(reads, 0, 1).reshape(tok_rows, local_heads, HEAD)
    center = mixer_out - jnp.mean(mixer_out, axis=-1, keepdims=True)
    spread = jnp.mean(center * center, axis=-1, keepdims=True)
    mixed = (
        (center * lax.rsqrt(spread + 1e-05) * head_norm_gain.reshape(local_heads, HEAD))
        .reshape(tok_rows, -1)
        .astype(jnp.bfloat16)
    )
    row_mixed = lax.all_to_all(mixed, "tp", split_axis=0, concat_axis=1, tiled=True)
    proj = jnp.dot(row_mixed, mixer_output_weight, preferred_element_type=jnp.float32)
    mid_f = (resid.astype(jnp.float32) + proj).astype(jnp.bfloat16).astype(jnp.float32)
    normed = (
        mid_f
        * lax.rsqrt(jnp.mean(mid_f * mid_f, axis=-1, keepdims=True) + 1e-06)
        * feedforward_norm_gain
    ).astype(jnp.bfloat16)
    whole_rows = gathered_copies(normed, "tp", 0)
    pieces = sent_together((gate_weight, up_weight), SP, 0, 1)
    gate = jnp.dot(whole_rows, pieces[0], preferred_element_type=jnp.float32)
    upper = jnp.dot(whole_rows, pieces[1], preferred_element_type=jnp.float32)
    whole_down = whole_of(down_weight, SP, 1)
    hidden = (jax.nn.silu(gate) * upper).astype(jnp.bfloat16)
    down_sum = sent_and_summed(
        jnp.dot(hidden, whole_down, preferred_element_type=jnp.float32).astype(jnp.bfloat16),
        "tp",
        0,
    )
    return (mid_f + 0.5 * down_sum).astype(jnp.bfloat16)


def solution(mesh):
    torus = Mesh(mesh.devices.reshape(8, 4, mesh.shape["tp"]), ("sp_0", "sp_1", "tp"))
    in_specs = (
        P(SP_TP, None),
        P(SP, "tp"),
        P(SP, "tp"),
        P(SP, "tp"),
        P(SP, "tp"),
        P("tp"),
        P(SP, "tp"),
        P(SP, "tp"),
        P("tp"),
        P("tp"),
        P(),
        P(),
        P(SP, "tp"),
        P(SP, "tp"),
        P("tp", SP),
    )
    out_specs = P(SP_TP, None)
    return jax.shard_map(
        per_device, mesh=torus, in_specs=in_specs, out_specs=out_specs, check_vma=False
    )
```

profile of v0, /device:TPU:1, one launch (start us, length us, event | category | flops | bytes accessed | tf_op | source)
XLA Modules:
  0.0 570.8 jit_solution(1547033450938407414)
XLA Ops:
  8.4 12.8 %all_gather.26 = bf16[704,256]{0,1:T(8,128)(2,1)} all-gather(bf16[704,64]{0,1:T(8,128)(2,1)} %param.31), channel_id=1, replica_groups=mesh['sp_0'=8,'sp_1'=4,'tp'=8] {'sp_1'}, dimensions={1}, use_global_device_ids=true | all-gather | bytes 450560 | tf_op jit(solution)/shard_map/all_gather | solution.py:87
  27.4 2.6 multiply_bitcast_fusion
  30.2 291.0 %while.17 = (s32[]{:T(128)}, f32[24,2,64,64]{3,2,1,0:T(8,128)S(1)}, f32[24,2,64,64]{3,2,1,0:T(8,128)S(1)}, f32[16,24,2,64]{3,0,2,1:T(8,128)}, f32[16,24,2,64]{3,...) while((s32[]{:T(128)}, f32[24,2,64,64]{3,2,1,0:T(8,128)S(1)}, ...), condition=%wide.region_2.3_spmd.clone, body=%wide.region_1.2_spmd.clone.sunk | while | flops 11409411 | bytes 6660256 | solution.py:183
  327.0 3.4 pad.59
  333.9 4.3 pad.62
  341.2 4.3 pad.61
  349.7 7.2 %pad.64 = f32[12,2,64,64]{3,2,1,0:T(8,128)} pad(f32[6,2,64,64]{3,2,1,0:T(8,128)} %copy-done.4, f32[]{:T(128)} %constant.26.clone.1), padding=1_0_1x0_0_0x0_0_0x0_0_0 | pad | bytes 589828 | tf_op jit(solution)/shard_map/pad | solution.py:184
  359.3 7.2 %pad.63 = f32[12,2,64,64]{3,2,1,0:T(8,128)} pad(f32[6,2,64,64]{3,2,1,0:T(8,128)} %pad_maximum_fusion.3, f32[]{:T(128)} %constant.26.clone.1), padding=0_1_1x0_0_0x0_0_0x0_0_0 | pad | bytes 589828 | tf_op jit(solution)/shard_map/pad | solution.py:184
  370.6 12.9 %pad.66 = f32[24,2,64,64]{3,2,1,0:T(8,128)} pad(f32[12,2,64,64]{3,2,1,0:T(8,128)} %copy-done.5, f32[]{:T(128)} %constant.26.clone.1), padding=1_0_1x0_0_0x0_0_0x0_0_0 | pad | bytes 1179652 | tf_op jit(solution)/shard_map/pad | solution.py:184
  385.8 2.6 pad.53
  390.0 4.6 pad.56
  395.3 4.6 pad.55
  404.0 8.6 %pad.65 = f32[24,2,64,64]{3,2,1,0:T(8,128)} pad(f32[12,2,64,64]{3,2,1,0:T(8,128)S(1)} %pad_maximum_fusion.1, f32[]{:T(128)} %constant.26.clone.1), padding=0_1_1x0_0_0x0_0_0x0_0_0 | pad | bytes 1179652 | tf_op jit(solution)/shard_map/pad | solution.py:184
  413.4 9.9 %all-gather = bf16[1024,64]{1,0:T(8,128)(2,1)S(1)} all-gather(bf16[256,64]{1,0:T(8,128)(2,1)S(1)} %pad_maximum_fusion.9), channel_id=2, replica_groups=mesh['sp_0'=8,'sp_1'=4,'tp'=8] {'sp_1'}, dimensions={0}, use_global_device_ids=true | all-gather | bytes 163840 | tf_op jit(solution)/shard_map/all_gather | solution.py:27
  424.7 22.4 %all-gather.1 = bf16[2048,64]{1,0:T(8,128)(2,1)S(1)} all-gather(bf16[256,64]{1,0:T(8,128)(2,1)S(1)} %pad_maximum_fusion.10), channel_id=3, replica_groups=mesh['sp_0'=8,'sp_1'=4,'tp'=8] {'sp_0'}, dimensions={0}, use_global_device_ids=true | all-gather | bytes 294912 | tf_op jit(solution)/shard_map/all_gather | solution.py:27
  451.1 8.8 %pad.93 = f32[23,2,64,64]{3,2,1,0:T(8,128)} pad(f32[12,2,64,64]{3,2,1,0:T(8,128)S(1)} %pad_maximum_fusion.1, f32[]{:T(128)} %constant.26.clone.1), padding=0_0_1x0_0_0x0_0_0x0_0_0 | pad | bytes 1146884 | tf_op jit(solution)/shard_map/slice | solution.py:187
  460.1 9.3 %pad.57 = f32[24,2,64,64]{3,2,1,0:T(8,128)S(1)} pad(f32[12,2,64,64]{3,2,1,0:T(8,128)} %pad_maximum_fusion, f32[]{:T(128)} %constant.26.clone.1), padding=0_1_1x0_0_0x0_0_0x0_0_0 | pad | bytes 1179652 | tf_op jit(solution)/shard_map/pad | solution.py:184
  472.7 2.6 fusion.105
  478.3 21.4 %all_to_all.26 = bf16[8,48,128]{2,1,0:T(8,128)(2,1)S(1)} all-to-all(bf16[8,48,128]{2,1,0:T(8,128)(2,1)S(1)} %multiply_convert_fusion.1), channel_id=1, replica_groups=mesh['sp_0'=8,'sp_1'=4,'tp'=8] {'tp'}, dimensions={0} | all-to-all | bytes 196608 | tf_op jit(solution)/shard_map/all_to_all | solution.py:205
  499.7 3.2 multiply_reduce_fusion
  503.2 23.8 %all_to_all.27 = bf16[8,48,2048]{2,1,0:T(8,128)(2,1)S(1)} all-to-all(bf16[8,48,2048]{2,1,0:T(8,128)(2,1)S(1)} %broadcast_in_dim.44), channel_id=1, replica_groups=mesh['sp_0'=8,'sp_1'=4,'tp'=8] {'tp'}, dimensions={0} | all-to-all | bytes 3145728 | tf_op jit(solution)/shard_map/all_to_all | solution.py:68
  527.0 4.6 fusion.8
  531.5 7.4 %convolution_convert_fusion = bf16[384,2048]{1,0:T(8,128)(2,1)S(1)} fusion(bf16[704,2048]{0,1:T(8,128)(2,1)} %all-gather.7.cloned.1.call-done, bf16[384,2048]{1,0:T(8,128)(2,1)S(1)} %bitcast.255, bf16[2048,1408]{1,0:T(8,128)(2,1)} %all-gather.5.cloned.1.call-done, f32[384,704]{0,1:T(8,128)} %fusion.8), kind=kOutput, calls=%fused_computation.21 | convolution fusion | flops 2217000960 | bytes 10518528 | tf_op jit(solution)/shard_map/dot_general | solution.py:220
  538.9 24.0 %all_to_all.28 = bf16[8,48,2048]{2,1,0:T(8,128)(2,1)S(1)} all-to-all(bf16[8,48,2048]{2,1,0:T(8,128)(2,1)S(1)} %bitcast.256), channel_id=1, replica_groups=mesh['sp_0'=8,'sp_1'=4,'tp'=8] {'tp'}, dimensions={0} | all-to-all | bytes 3145728 | tf_op jit(solution)/shard_map/all_to_all | solution.py:98
  (378 shorter events, 343.5 us)
Async XLA Ops:
  6.5 17.1 %copy-start.33 = (bf16[384,128]{1,0:T(8,128)(2,1)S(1)}, bf16[384,128]{1,0:T(8,128)(2,1)}, u32[]{:S(2)}) copy-start(bf16[384,128]{1,0:T(8,128)(2,1)} %param.21) | copy-start | bytes 294916
  6.5 17.1 %copy-start.39 = (f32[128]{0:T(128)S(1)}, f32[128]{0:T(128)}, u32[]{:S(2)}) copy-start(f32[128]{0:T(128)} %param.22) | copy-start | bytes 1540
  6.5 520.4 %all-gather.5.cloned.1.call-start = ((), (), s32[]{:S(2)}) async-start(), calls=%async_computation.3 | async-start | bytes 5947392 | tf_op jit(solution)/shard_map/all_gather | solution.py:77
  8.3 15.8 %copy-start.38 = (f32[384,2]{0,1:T(2,128)S(1)}, f32[384,2]{0,1:T(2,128)}, u32[]{:S(2)}) copy-start(f32[384,2]{0,1:T(2,128)} %param.23) | copy-start | bytes 9220
  8.3 523.2 %all-gather.7.cloned.1.call-start = ((), (), s32[]{:S(2)}) async-start(), calls=%async_computation.4 | async-start | bytes 3538944 | tf_op jit(solution)/shard_map/all_gather | solution.py:87
  21.2 3.1 copy-start.34
  21.2 3.1 copy-start.40
  22.3 3.1 copy-start.35
  22.5 7.6 %copy-start.11 = (f32[64,64]{1,0:T(8,128)}, f32[64,64]{1,0:T(8,128)S(1)}, u32[]{:S(2)}) copy-start(f32[64,64]{1,0:T(8,128)S(1)} %fusion.84) | copy-start | bytes 49156
  22.5 3.9 copy-start.36
  370.6 12.9 %copy-start.9 = (f32[3,2,64,64]{3,2,1,0:T(8,128)S(1)}, f32[3,2,64,64]{3,2,1,0:T(8,128)}, u32[]{:S(2)}) copy-start(f32[3,2,64,64]{3,2,1,0:T(8,128)} %copy-done.8) | copy-start | bytes 294916
  370.6 13.9 %slice-start.1 = ((f32[3,2,64,64]{3,2,1,0:T(8,128)}), f32[1,2,64,64]{3,2,1,0:T(8,128)S(1)}, s32[]{:S(2)}) async-start(f32[3,2,64,64]{3,2,1,0:T(8,128)} %copy-done.8), calls=%async_computation.6 | async-start | bytes 131072 | tf_op jit(solution)/shard_map/slice | solution.py:184
  384.6 4.9 copy-start.1
  388.5 6.8 %slice-start = ((f32[12,2,64,64]{3,2,1,0:T(8,128)}), f32[1,2,64,64]{3,2,1,0:T(8,128)S(1)}, s32[]{:S(2)}) async-start(f32[12,2,64,64]{3,2,1,0:T(8,128)} %copy-done), calls=%async_computation.5 | async-start | bytes 131072 | tf_op jit(solution)/shard_map/slice | solution.py:184
  394.6 5.3 copy-start.7
  404.0 19.4 %copy-start.12 = (f32[64,64]{1,0:T(8,128)S(1)}, f32[64,64]{1,0:T(8,128)}, u32[]{:S(2)}) copy-start(f32[64,64]{1,0:T(8,128)} %copy-done.11) | copy-start | bytes 49156
  423.5 24.5 %copy-start.17 = (f32[1,2,64,64]{3,2,1,0:T(8,128)S(1)}, f32[1,2,64,64]{3,2,1,0:T(8,128)}, u32[]{:S(2)}) copy-start(f32[1,2,64,64]{3,2,1,0:T(8,128)} %slice.260) | copy-start | bytes 98308
  448.0 2.0 copy-start.21
  448.0 2.0 copy-start.22
  448.0 2.1 copy-start.20
  469.7 1.9 copy-start.3
  476.4 1.9 copy-start.41
  477.0 22.6 %copy-start.19 = (bf16[48,2048]{1,0:T(8,128)(2,1)S(1)}, bf16[48,2048]{1,0:T(8,128)(2,1)}, u32[]{:S(2)}) copy-start(bf16[48,2048]{1,0:T(8,128)(2,1)} %param.17) | copy-start | bytes 589828
  499.7 3.2 copy-start.37
  (22 other events, 28.5 us)
Sparse Core Ops, SparseCore 0:
  9.9 88.5 all-gather.4
  100.3 42.9 all-gather.6
where the time goes:
time: 581 us; the launch traced here: 571 us
  matrix products  197 us (34%)
  local copies, waits for them, and re-layouts  187 us (32%)
  blocking collectives  114 us (20%)
  other arithmetic  58 us (10%)
  between operations  14.5 us (2%)
    pad x14, local copies, waits for them, and re-layouts, per_device(): inclusive = lax.associative_scan(combine, (end_trans, end_state), axis=0)  69.4 us
    dynamic_update_slice x32, local copies, waits for them, and re-layouts, per_device(): lax.scan(block_step, start, step_inputs)  54.3 us
    dot_general x16, matrix products, block_step(): jnp.einsum('bhjk,bhk->bhj', trans, lifted, precision=lax.Precision.HIGHEST)  40.9 us
    dot_general x16, matrix products, block_step(): jnp.einsum('bhvk,bhk->bhv', state, lifted, precision=lax.Precision.HIGHEST)  40.8 us
    dot_general x16, matrix products, block_step(): jnp.einsum('bhjk,bhk->bhj', trans, query_t, precision=lax.Precision.HIGHEST)  40.6 us
    dot_general x16, matrix products, block_step(): jnp.einsum('bhvk,bhk->bhv', state, query_t, precision=lax.Precision.HIGHEST)  40.6 us
    all_gather x2, blocking collectives, gathered_once(): both, at, found = (lax.all_gather(jnp.concatenate(lines), axis), 0, {})  32.3 us
    add x16, other arithmetic, block_step(): trans * decay_t[:, :, None, :]  24.8 us
  transfers between devices with their start and end apart: 2, of which 0 were waited for; matrix products, arithmetic and copies ran while one was open for 75% of the time, Pallas kernels for 0%

commit v1 on v0

v1 whole, which is shorter than its diff:
```python
import functools

import jax
import jax.numpy as jnp
from jax import lax
from jax.experimental import pallas as pl
from jax.experimental.pallas import tpu as pltpu
from jax.sharding import Mesh
from jax.sharding import PartitionSpec as P

F32, BF16 = jnp.float32, jnp.bfloat16
MESH = pl.DeviceIdType.MESH
HEAD, LANES, CH = 64, 128, 64
NZ, NX, NY, NC = 8, 4, 4, 2
NT = NY * NC
CHUNKS = 6
GROUP = 3
COLS = 4
SP, TP, SP_TP = ("z", "x"), ("y", "c"), ("z", "x", "y", "c")


def dg(a, b, ca=1, cb=0):
    return lax.dot_general(a, b, (((ca,), (cb,)), ((), ())), preferred_element_type=F32)


def halves(x):
    hi = x.astype(BF16)
    return hi, (x - hi.astype(F32)).astype(BF16)


def mm(a, b, ca=1, cb=0):
    return dg(a[0], b[0], ca, cb) + dg(a[0], b[1], ca, cb) + dg(a[1], b[0], ca, cb)


def thirds(x):
    hi = x.astype(BF16)
    rest = x - hi.astype(F32)
    mid = rest.astype(BF16)
    return hi, mid, (rest - mid.astype(F32)).astype(BF16)


def iota(shape, dim):
    return lax.broadcasted_iota(jnp.int32, shape, dim)


def first_head(rows):
    return iota((rows, LANES), 1) < HEAD


def stacked(x):
    own = first_head(x.shape[0])
    zero = jnp.zeros_like(x)
    return jnp.concatenate([jnp.where(own, x, zero), jnp.where(own, zero, x)], axis=0)


def folded(x):
    half = x.shape[0] // 2
    return x[:half] + x[half:]


def head_ones():
    return (iota((LANES, LANES), 0) // HEAD == iota((LANES, LANES), 1) // HEAD).astype(BF16)


def head_sum(x, ones):
    hi, lo = halves(x)
    return dg(hi, ones) + dg(lo, ones)


def sigmoid(x):
    return 1.0 / (1.0 + jnp.exp(-x))


def mixer_group(first, q_ref, k_ref, v_ref, dip_ref, cri_ref, dco_ref, cro_ref, extra_ref, m_ref, n_ref, r_ref, o_ref):
    ids = range(first, first + GROUP)
    ones = head_ones()
    row, col = iota((LANES, LANES), 0), iota((LANES, LANES), 1)
    eye = (row == col).astype(F32)
    low = (iota((CH, CH), 0) >= iota((CH, CH), 1)).astype(BF16)
    ends, us, bts, avs, reads, vs = [], [], [], [], [], []
    invs, offs, qks = [], [], []
    for c in ids:
        rows = pl.ds(c * CH, CH)
        q, k, v = (r[rows, :].astype(F32) for r in (q_ref, k_ref, v_ref))
        pre = dco_ref[...] + dip_ref[rows, :].astype(F32)
        log_decay = -(sigmoid(pre) * 0.6065306597126334) - extra_ref[rows, :]
        unit = k * lax.rsqrt(head_sum(k * k, ones) + 1e-6)
        b = unit * sigmoid(cro_ref[...] + cri_ref[rows, :].astype(F32))
        total = sum(dg(low, part) for part in thirds(log_decay))
        before = total - log_decay
        mid, end = total[CH // 2 - 1 : CH // 2], total[CH - 1 :]
        up, down = jnp.exp(total - mid), jnp.exp(mid - total)
        up_before = jnp.exp(before - mid)
        rest = jnp.exp(end - total)
        left = halves(jnp.concatenate([stacked(unit * up_before), stacked(q * up)], axis=0))
        right = halves(jnp.concatenate([stacked(k * down), stacked(b * down)], axis=0))
        a = mm(left, right, 1, 1)
        a_uk = jnp.where(row > col, a[:LANES, :LANES], 0.0)
        a_qk = jnp.where(row >= col, a[LANES:, :LANES], 0.0)
        a_qb = jnp.where(row >= col, a[LANES:, LANES:], 0.0)
        offs.append(a[:LANES, LANES:])
        vst = halves(stacked(v))
        av = mm(halves(jnp.concatenate([a_uk, a_qk], axis=0)), vst)
        us.append(halves(jnp.concatenate([stacked(unit * jnp.exp(before)), av[:LANES]], axis=1)))
        avs.append(av[LANES:])
        qks.append(halves(a_qb))
        reads.append(stacked(q * jnp.exp(total)))
        bts.append(halves(stacked(b * rest)))
        ends.append((jnp.exp(end), mm(vst, halves(stacked(k * rest)), 0, 0)))
    size = 1
    while size < CH:
        inside = (row // (2 * size) == col // (2 * size)) & (row // size != col // size) & (row > col)
        for i in range(GROUP):
            part = jnp.where(inside, offs[i], 0.0)
            if size == 1:
                invs.append(eye - part)
            else:
                inv = halves(invs[i])
                invs[i] = invs[i] - mm(halves(mm(inv, halves(part))), inv)
        size *= 2
    for i, c in enumerate(ids):
        wu = mm(halves(invs[i]), us[i])
        wu2 = halves(wu)
        ro = mm(qks[i], wu2)
        r_ref[c] = reads[i] - ro[:, :LANES]
        o_ref[c] = avs[i] - ro[:, LANES:]
        mn = mm(wu2, bts[i], 0, 0)
        decay, kv = ends[i]
        m_ref[c] = jnp.where(row == col, decay, 0.0) - mn[:LANES]
        n_ref[c] = kv - mn[LANES:]


def unpacked(message):
    wide = message.astype(F32)
    return stacked(wide[:HEAD]).astype(BF16), stacked(wide[HEAD:])


def packed(trans, state):
    return jnp.concatenate([folded(trans), folded(state)], axis=0).astype(BF16)


def after(total, message):
    trans, state = unpacked(message)
    hi, lo = halves(total)
    out = dg(hi, trans) + dg(lo, trans)
    return jnp.concatenate([out[:LANES], out[LANES:] + state], axis=0)


class Gather:
    def __init__(self, bufs, send_z, recv_z, send_x, recv_x, sends):
        self.bufs, self.sends = bufs, sends
        self.send_z, self.recv_z, self.send_x, self.recv_x = send_z, recv_z, send_x, recv_x
        self.z, self.x = lax.axis_index("z"), lax.axis_index("x")

    def at(self, w, dz, dx, part=None):
        ref = self.bufs[w].at[lax.rem(self.z + dz + NZ, NZ), lax.rem(self.x + dx + NX, NX)]
        rows = ref.shape[0] // 2
        return ref if part is None else ref.at[pl.ds(part * rows, rows)]

    def along_z(self, ring, w, dx, hop, right):
        sign = 1 if right else -1
        part = None if hop < 4 else (0 if right else 1)
        ref = self.at(w, -sign * (hop - 1), dx, part)
        slot = hop - 1 + (0 if right else 4)
        return pltpu.make_async_remote_copy(
            ref, ref, self.send_z.at[ring, slot], self.recv_z.at[ring, slot],
            device_id={"z": lax.rem(self.z + sign + NZ, NZ)}, device_id_type=MESH,
        )

    def got_z(self, ring, w, dx, hop, right):
        sign = 1 if right else -1
        part = None if hop < 4 else (0 if right else 1)
        ref = self.at(w, -sign * hop, dx, part)
        slot = hop - 1 + (0 if right else 4)
        pltpu.make_async_remote_copy(
            ref, ref, self.send_z.at[ring, slot], self.recv_z.at[ring, slot],
            device_id={"z": lax.rem(self.z + sign + NZ, NZ)}, device_id_type=MESH,
        ).wait_recv()

    def along_x(self, ring, w, dz, hop, right):
        sign = 1 if right else -1
        part = None if hop < 2 else (0 if right else 1)
        ref = self.at(w, dz, -sign * (hop - 1), part)
        slot = hop - 1 + (0 if right else 2)
        return pltpu.make_async_remote_copy(
            ref, ref, self.send_x.at[ring, slot], self.recv_x.at[ring, slot],
            device_id={"x": lax.rem(self.x + sign + NX, NX)}, device_id_type=MESH,
        )

    def got_x(self, ring, w, dz, hop, right):
        sign = 1 if right else -1
        part = None if hop < 2 else (0 if right else 1)
        ref = self.at(w, dz, -sign * hop, part)
        slot = hop - 1 + (0 if right else 2)
        pltpu.make_async_remote_copy(
            ref, ref, self.send_x.at[ring, slot], self.recv_x.at[ring, slot],
            device_id={"x": lax.rem(self.x + sign + NX, NX)}, device_id_type=MESH,
        ).wait_recv()

    def go(self, copy):
        copy.start()
        self.sends.append(copy)

    def z_hop(self, ring, w, dx, hop):
        for right in (True, False):
            self.go(self.along_z(ring, w, dx, hop, right))

    def x_hop(self, ring, w, dz, hop):
        for right in (True, False):
            self.go(self.along_x(ring, w, dz, hop, right))

    def z_got(self, ring, w, dx, hop):
        for right in (True, False):
            self.got_z(ring, w, dx, hop, right)

    def x_got(self, ring, w, dz, hop):
        for right in (True, False):
            self.got_x(ring, w, dz, hop, right)


DZ = (0, -1, 1, -2, 2, -3, 3, 4)
DX = (0, 1, -1, 2)


def stages(g):
    def start():
        for w, ring in ((1, 0), (2, 1)):
            g.z_hop(ring, w, 0, 1)
        g.x_hop(16, 0, 0, 1)
        g.z_hop(2, 0, 0, 1)
        for w in (1, 2):
            g.x_hop(8 * (w - 1), w, 0, 1)

    def z_round(hop):
        for w, ring in ((1, 0), (2, 1)):
            g.z_got(ring, w, 0, hop)
            if hop < 4:
                g.z_hop(ring, w, 0, hop + 1)
                for i in (2 * hop - 1, 2 * hop):
                    g.x_hop(8 * (w - 1) + i, w, DZ[i], 1)
            else:
                g.x_hop(8 * (w - 1) + 7, w, 4, 1)

    def x_first():
        g.x_got(16, 0, 0, 1)
        g.x_hop(16, 0, 0, 2)
        for i in (1, 2):
            g.z_hop(2 + i, 0, DX[i], 1)

    def x_second():
        g.x_got(16, 0, 0, 2)
        g.z_hop(5, 0, 2, 1)

    def x_forward(i):
        for w in (1, 2):
            g.x_got(8 * (w - 1) + i, w, DZ[i], 1)
            g.x_hop(8 * (w - 1) + i, w, DZ[i], 2)

    def g_round(i, hop):
        g.z_got(2 + i, 0, DX[i], hop)
        if hop < 4:
            g.z_hop(2 + i, 0, DX[i], hop + 1)

    def x_last(i):
        for w in (1, 2):
            g.x_got(8 * (w - 1) + i, w, DZ[i], 2)

    return start, z_round, x_first, x_second, x_forward, g_round, x_last


def kernel(
    q_ref, k_ref, v_ref, dip_ref, cri_ref, dco_ref, cro_ref, gain_ref, extra_ref, fng_ref,
    resid_hbm, wo_hbm, gate_hbm, up_hbm, down_hbm,
    out_ref,
    wg, wu, wd, wo, resid,
    m_ref, n_ref, r_ref, o_ref, gm_ref, hm_ref,
    tot_ref, xbuf, xpre, zsrc, zbuf, s_ref,
    mixed_ref, rowmix, mid_ref, rows, hid_ref,
    own_part, full_part, sib_src, sib_buf, y_src, y_buf,
    local_sem, send_z, recv_z, send_x, recv_x,
    st_send, st_recv, a2a_send, a2a_recv, ag_send, ag_recv, rs_send, rs_recv,
):
    z, x, y, c = (lax.axis_index(n) for n in SP_TP)
    tp = y * NC + c
    sends = []
    own = [
        pltpu.make_async_copy(src, dst, local_sem.at[i])
        for i, (src, dst) in enumerate(
            ((up_hbm, wu.at[z, x]), (down_hbm, wd.at[z, x]), (gate_hbm, wg.at[z, x]), (wo_hbm, wo), (resid_hbm, resid))
        )
    ]
    for copy in own:
        copy.start()

    barrier = pltpu.get_barrier_semaphore()
    peers = [{"x": lax.rem(x + d, NX)} for d in range(1, NX)]
    peers += [{"z": lax.rem(z + d, NZ)} for d in range(1, NZ)]
    peers += [{"y": lax.rem(tp + d, NT) // NC, "c": lax.rem(tp + d, NT) % NC} for d in range(1, NT)]
    for peer in peers:
        pl.semaphore_signal(barrier, inc=1, device_id=peer, device_id_type=MESH)
    pl.semaphore_wait(barrier, len(peers))

    g = Gather((wg, wu, wd), send_z, recv_z, send_x, recv_x, sends)
    start, z_round, x_first, x_second, x_forward, g_round, x_last = stages(g)
    for copy in own[:3]:
        copy.wait()
    start()

    mix = functools.partial(
        mixer_group, q_ref=q_ref, k_ref=k_ref, v_ref=v_ref, dip_ref=dip_ref, cri_ref=cri_ref, dco_ref=dco_ref,
        cro_ref=cro_ref, extra_ref=extra_ref, m_ref=m_ref, n_ref=n_ref, r_ref=r_ref, o_ref=o_ref,
    )
    mix(0)
    x_first()
    z_round(1)
    mix(GROUP)
    x_second()
    z_round(2)

    row, col = iota((LANES, LANES), 0), iota((LANES, LANES), 1)
    total = jnp.concatenate([(row == col).astype(F32), jnp.zeros((LANES, LANES), F32)], axis=0)
    for i in range(CHUNKS):
        split = halves(total)
        gh = mm(halves(r_ref[i]), split, 1, 1)
        rows_i = pl.ds(i * CH, CH)
        gm_ref[rows_i, :] = folded(gh[:, :LANES])
        hm_ref[rows_i, :] = folded(gh[:, LANES:] + o_ref[i])
        step = mm(split, halves(m_ref[i]))
        total = jnp.concatenate([step[:LANES], step[LANES:] + n_ref[i]], axis=0)
    tot_ref[...] = packed(total[:LANES], total[LANES:])
    for d in range(1, NX):
        copy = pltpu.make_async_remote_copy(
            tot_ref, xbuf.at[d - 1], st_send.at[d - 1], st_recv.at[d - 1],
            device_id={"x": lax.rem(x + d, NX)}, device_id_type=MESH,
        )
        copy.start()
        sends.append(copy)
    x_forward(0)
    for d in range(1, NX):
        pltpu.make_async_remote_copy(
            tot_ref, xbuf.at[d - 1], st_send.at[d - 1], st_recv.at[d - 1],
            device_id={"x": lax.rem(x + d, NX)}, device_id_type=MESH,
        ).wait_recv()
    total = jnp.concatenate([(row == col).astype(F32), jnp.zeros((LANES, LANES), F32)], axis=0)
    prefix = total
    for i in range(NX):
        prefix = jnp.where(x == i, total, prefix)
        message = tot_ref[...]
        for d in range(1, NX):
            message = jnp.where(lax.rem(x - i + NX, NX) == d, xbuf[d - 1], message)
        total = after(total, message)
    xpre[...] = prefix
    zsrc[...] = packed(total[:LANES], total[LANES:])

    def z_state(d):
        return pltpu.make_async_remote_copy(
            zsrc, zbuf.at[d - 1], st_send.at[2 + d], st_recv.at[2 + d],
            device_id={"z": lax.rem(z + d, NZ)}, device_id_type=MESH,
        )

    for d in range(1, NZ):
        pl.when(z + d < NZ)(lambda d=d: z_state(d).start())
    z_round(3)
    s_ref[...] = jnp.zeros_like(s_ref)
    for d in range(NZ - 1, 0, -1):

        @pl.when(z >= d)
        def _(d=d):
            z_state(d).wait_recv()
            trans, state = unpacked(zbuf[d - 1])
            hi, lo = halves(s_ref[...])
            s_ref[...] = dg(hi, trans) + dg(lo, trans) + state

    incoming = mm(halves(s_ref[...]), halves(xpre[:LANES])) + xpre[LANES:]
    read = mm(halves(gm_ref[...]), halves(incoming), 1, 1) + hm_ref[...]
    ones = head_ones()
    center = read - head_sum(read, ones) * (1.0 / HEAD)
    spread = head_sum(center * center, ones) * (1.0 / HEAD)
    mixed_ref[...] = (center * lax.rsqrt(spread + 1e-5) * gain_ref[...]).astype(BF16)

    share = mixed_ref.shape[0] // NT
    mine = pl.ds(pl.multiple_of(tp * LANES, LANES), LANES)

    def to_row(d):
        other = lax.rem(tp + d, NT)
        part = mixed_ref.at[pl.ds(pl.multiple_of(other * share, 16), share)]
        return pltpu.make_async_remote_copy(
            part, rowmix.at[:, mine], a2a_send.at[d - 1], a2a_recv.at[d - 1],
            device_id={"y": other // NC, "c": other % NC}, device_id_type=MESH,
        )

    for d in range(1, NT):
        copy = to_row(d)
        copy.start()
        sends.append(copy)
    rowmix[:, mine] = mixed_ref[pl.ds(pl.multiple_of(tp * share, 16), share), :]
    z_round(4)
    for copy in own[3:]:
        copy.wait()
    for d in range(1, NT):
        to_row(d).wait_recv()

    width = 512
    square = jnp.zeros((share, 1), F32)
    for i in range(mid_ref.shape[1] // width):
        cols = pl.ds(i * width, width)
        proj = jnp.dot(rowmix[...], wo[:, cols], preferred_element_type=F32)
        mid = (resid[:, cols].astype(F32) + proj).astype(BF16)
        mid_ref[:, cols] = mid
        mid = mid.astype(F32)
        square += jnp.sum(mid * mid, axis=-1, keepdims=True)
    scale = lax.rsqrt(square * (1.0 / mid_ref.shape[1]) + 1e-6)
    for i in range(mid_ref.shape[1] // width):
        cols = pl.ds(i * width, width)
        rows[tp, :, cols] = (mid_ref[:, cols].astype(F32) * scale * fng_ref[:, cols]).astype(BF16)

    half = mid_ref.shape[1] // 2

    def y_rows(sem, dy, to, cols):
        ref = rows.at[lax.rem(y + dy + NY, NY) * NC + c, :, cols]
        return pltpu.make_async_remote_copy(
            ref, ref, ag_send.at[sem], ag_recv.at[sem], device_id={"y": lax.rem(y + to + NY, NY)}, device_id_type=MESH
        )

    def c_rows(sem, dy, mate):
        ref = rows.at[lax.rem(y + dy + NY, NY) * NC + (1 - c if mate else c)]
        return pltpu.make_async_remote_copy(
            ref, ref, ag_send.at[sem], ag_recv.at[sem], device_id={"c": 1 - c}, device_id_type=MESH
        )

    def go(copy):
        copy.start()
        sends.append(copy)

    every, left, right = pl.ds(0, 2 * half), pl.ds(0, half), pl.ds(half, half)
    go(y_rows(0, 0, 1, every))
    go(y_rows(1, 0, -1, every))
    go(c_rows(4, 0, False))
    x_forward(1)
    x_forward(2)
    y_rows(0, -1, 1, every).wait_recv()
    go(y_rows(2, -1, 1, left))
    go(c_rows(5, -1, False))
    y_rows(1, 1, -1, every).wait_recv()
    go(y_rows(3, 1, -1, right))
    go(c_rows(6, 1, False))
    for i in range(3):
        g_round(i, 1)
    y_rows(2, 2, 1, left).wait_recv()
    y_rows(3, 2, -1, right).wait_recv()
    go(c_rows(7, 2, False))
    for sem, dy in ((4, 0), (5, -1), (6, 1), (7, 2)):
        c_rows(sem, dy, True).wait_recv()

    x_forward(3)
    x_forward(4)
    g_round(3, 1)
    for i in range(4):
        g_round(i, 2)
    x_forward(5)
    x_forward(6)
    for i in range(4):
        g_round(i, 3)
    x_forward(7)
    x_last(0)
    for i in range(4):
        g_round(i, 4)
    for i in range(1, 8):
        x_last(i)

    tokens = NT * share
    depth, hidden = NZ * NX * wg.shape[2], wg.shape[3]
    token_rows = rows[...].reshape(tokens, depth)
    gate = jnp.dot(token_rows, wg[...].reshape(depth, hidden), preferred_element_type=F32)
    upper = jnp.dot(token_rows, wu[...].reshape(depth, hidden), preferred_element_type=F32)
    hid_ref[...] = (gate * sigmoid(gate) * upper).astype(BF16)

    def to_mate(n):
        return pltpu.make_async_remote_copy(
            sib_src.at[n], sib_buf.at[n], rs_send.at[n], rs_recv.at[n], device_id={"c": 1 - c}, device_id_type=MESH
        )

    def to_y(n, d):
        sem = COLS + n * (NY - 1) + d - 1
        return pltpu.make_async_remote_copy(
            y_src.at[n, d - 1], y_buf.at[n, d - 1], rs_send.at[sem], rs_recv.at[sem],
            device_id={"y": lax.rem(y + d, NY)}, device_id_type=MESH,
        )

    def chip_sum(n):
        to_mate(n).wait_recv()
        for d in range(NY):
            yy = lax.rem(y + d, NY)
            both = full_part[n, pl.ds(pl.multiple_of((yy * NC + c) * share, 16), share), :] + sib_buf[n, yy].astype(F32)
            if d == 0:
                own_part[n] = both
            else:
                y_src[n, d - 1] = both.astype(BF16)
                go(to_y(n, d))

    step = NZ // COLS
    for n in range(COLS):
        weights = wd[n * step : (n + 1) * step].reshape(depth // COLS, hidden)
        full_part[n] = dg(hid_ref[...], weights, 1, 1)
        for yy in range(NY):
            sib_src[n, yy] = full_part[n, pl.ds(pl.multiple_of((yy * NC + 1 - c) * share, 16), share), :].astype(BF16)
        go(to_mate(n))
        if n:
            chip_sum(n - 1)
    chip_sum(COLS - 1)
    wide = depth // COLS
    for n in range(COLS):
        acc = own_part[n]
        for d in range(1, NY):
            to_y(n, d).wait_recv()
            acc += y_buf[n, d - 1].astype(F32)
        cols = pl.ds(n * wide, wide)
        out_ref[:, cols] = (mid_ref[:, cols].astype(F32) + 0.5 * acc).astype(BF16)

    for copy in sends:
        copy.wait_send()
    for d in range(1, NZ):
        pl.when(z + d < NZ)(lambda d=d: z_state(d).wait_send())


def per_device(
    resid, queries, keys, values, decay_input_part, decay_channel_offset, decay_head_extra, correction_rate_input,
    correction_rate_offset, head_norm_gain, mixer_output_weight, feedforward_norm_gain, gate_weight, up_weight, down_weight,
):
    tokens = queries.shape[0]
    share, width = resid.shape
    shard, hidden = gate_weight.shape
    extra = jnp.repeat(decay_head_extra, HEAD, axis=1)
    vm, sem = pltpu.VMEM, pltpu.SemaphoreType.DMA
    flat = pl.BlockSpec(memory_space=pltpu.VMEM)
    there = pl.BlockSpec(memory_space=pl.ANY)
    wide = width // COLS
    weights = vm((NZ, NX, shard, hidden), BF16)
    return pl.pallas_call(
        kernel,
        name="layer",
        out_shape=jax.ShapeDtypeStruct((share, width), BF16),
        in_specs=[flat] * 10 + [there] * 5,
        out_specs=flat,
        scratch_shapes=[
            weights, weights, weights, vm(mixer_output_weight.shape, BF16), vm((share, width), BF16),
            vm((CHUNKS, LANES, LANES), F32), vm((CHUNKS, LANES, LANES), F32),
            vm((CHUNKS, LANES, LANES), F32), vm((CHUNKS, LANES, LANES), F32),
            vm((tokens, LANES), F32), vm((tokens, LANES), F32),
            vm((LANES, LANES), BF16), vm((NX - 1, LANES, LANES), BF16), vm((2 * LANES, LANES), F32),
            vm((LANES, LANES), BF16), vm((NZ - 1, LANES, LANES), BF16), vm((LANES, LANES), F32),
            vm((tokens, LANES), BF16), vm((share, NT * LANES), BF16), vm((share, width), BF16),
            vm((NT, share, width), BF16), vm((tokens, hidden), BF16),
            vm((COLS, share, wide), F32), vm((COLS, tokens, wide), F32),
            vm((COLS, NY, share, wide), BF16), vm((COLS, NY, share, wide), BF16),
            vm((COLS, NY - 1, share, wide), BF16), vm((COLS, NY - 1, share, wide), BF16),
            sem((5,)), sem((6, 8)), sem((6, 8)), sem((17, 4)), sem((17, 4)),
            sem((NX + NZ - 2,)), sem((NX + NZ - 2,)), sem((NT - 1,)), sem((NT - 1,)), sem((8,)), sem((8,)),
            sem((COLS * NY,)), sem((COLS * NY,)),
        ],
        compiler_params=pltpu.CompilerParams(collective_id=0, has_side_effects=True),
    )(
        queries, keys, values, decay_input_part, correction_rate_input,
        decay_channel_offset[None], correction_rate_offset[None], head_norm_gain[None], extra,
        feedforward_norm_gain[None], resid, mixer_output_weight, gate_weight, up_weight, down_weight.T,
    )


def solution(mesh):
    torus = Mesh(mesh.devices.reshape(NZ, NX, NY, NC), SP_TP)
    in_specs = (
        P(SP_TP, None), P(SP, TP), P(SP, TP), P(SP, TP), P(SP, TP), P(TP), P(SP, TP), P(SP, TP), P(TP), P(TP),
        P(), P(), P(SP, TP), P(SP, TP), P(TP, SP),
    )
    return jax.shard_map(per_device, mesh=torus, in_specs=in_specs, out_specs=P(SP_TP, None), check_vma=False)
```

time: 581 us -> 108 us (0.19); the launches traced: 571 us -> 108 us
  matrix products: 197 us -> 0 us
  local copies, waits for them, and re-layouts: 187 us -> 3.12 us
  blocking collectives: 114 us -> 0 us
  Pallas kernels: 0 us -> 105 us
  other arithmetic: 58 us -> 0 us
  between operations: 14.5 us -> 0.01 us
    dot_general x104 -> x0, matrix products: 197 us -> none  [the longest x16 40.9 us: block_step(): jnp.einsum('bhjk,bhk->bhj', trans, lifted, precision=lax.Precision.HIGHEST)]
    pallas_call x0 -> x1, Pallas kernels: none -> 105 us  [per_device(): pl.pallas_call(kernel, name='layer', out_shape=jax.ShapeDtypeStruct((shar...]
    pad x14 -> x0, local copies, waits for them, and re-layouts: 69.4 us -> none  [per_device(): inclusive = lax.associative_scan(combine, (end_trans, end_state), axis=0)]
    all_to_all x3 -> x0, blocking collectives: 69.2 us -> none  [the longest x1 24 us: sent_and_summed(): lax.all_to_all(cut_along(array, dim, count), axis, 0, 0, tiled=True)]
    dynamic_update_slice x32 -> x0, local copies, waits for them, and re-layouts: 54.3 us -> none  [per_device(): lax.scan(block_step, start, step_inputs)]
    all_gather x3 -> x0, blocking collectives: 45.1 us -> none  [the longest x2 32.3 us: gathered_once(): both, at, found = (lax.all_gather(jnp.concatenate(lines), axis), 0, {})]
    add x24 -> x0, other arithmetic: 31.3 us -> none  [the longest x16 24.8 us: block_step(): trans * decay_t[:, :, None, :]]
    mul x34 -> x0, local copies, waits for them, and re-layouts: 24.9 us -> none  [the longest x16 12.3 us: block_step(): value_t[..., None] * key_t[:, :, None, :]]
  transfers between devices with their start and end apart: 2 -> 0, of which waited for: 0 -> 0; matrix products, arithmetic and copies ran while one was open for 75% -> 0% of each run, Pallas kernels for 0% -> 0%
where the time goes in v1:
time: 108 us
  Pallas kernels  105 us (97%)
  local copies, waits for them, and re-layouts  3.12 us (3%)
    pallas_call x1, Pallas kernels, per_device(): pl.pallas_call(kernel, name='layer', out_shape=jax.ShapeDtypeStruct((shar...  105 us

profile of v1, /device:TPU:1, one launch (start us, length us, event | category | flops | bytes accessed | tf_op | source)
XLA Modules:
  0.0 107.9 jit_solution(5283258944015722834)
XLA Ops:
  0.0 0.7 broadcast_in_dim.18
  0.7 0.8 copy.17.extra_ref
  1.5 104.8 %layer.1 = bf16[48,2048]{1,0:T(8,128)(2,1)} custom-call(bf16[384,128]{1,0:T(8,128)(2,1)} %q_ref.1, bf16[384,128]{1,0:T(8,128)(2,1)} %k_ref.1, bf16[384,128]{1,0:T(8,128)(2,1)} %v_ref.1, bf16[384,128]{1,0:T(8,128)(2,1)} %dip_ref.1, bf16[384,128]{1,0:T(8,128)(2,1)} %cri_ref.1, f32[1,128]{1,0:T(1,128)} %bitcast.9, f32[1,128]{1,0:T(1,128)} %bitcast.10, ...), custom_call_target="tpu_custom_call" | custom-call | tf_op jit(solution)/shard_map/layer/pallas_call | solution.py:539
  106.3 1.6 %copy.19 = bf16[48,2048]{1,0:T(8,128)(2,1)} copy(bf16[48,2048]{1,0:T(8,128)(2,1)} %layer.1) | data formatting | bytes 393216

commit v2 on v1

v2 whole, which is shorter than its diff:
```python
import functools

import jax
import jax.numpy as jnp
from jax import lax
from jax.experimental import pallas as pl
from jax.experimental.pallas import tpu as pltpu
from jax.sharding import Mesh
from jax.sharding import PartitionSpec as P

F32, BF16 = jnp.float32, jnp.bfloat16
MESH = pl.DeviceIdType.MESH
HEAD, LANES, CH = 64, 128, 64
NZ, NX, NY, NC = 8, 4, 4, 2
NT = NY * NC
CHUNKS = 6
GROUP = 3
COLS = ((0, 1, 2), (3, 4), (5, 6), (7,))
SP, TP, SP_TP = ("z", "x"), ("y", "c"), ("z", "x", "y", "c")


def dg(a, b, ca=1, cb=0):
    return lax.dot_general(a, b, (((ca,), (cb,)), ((), ())), preferred_element_type=F32)


def halves(x):
    hi = x.astype(BF16)
    return hi, (x - hi.astype(F32)).astype(BF16)


def mm(a, b, ca=1, cb=0):
    return dg(a[0], b[0], ca, cb) + dg(a[0], b[1], ca, cb) + dg(a[1], b[0], ca, cb)


def thirds(x):
    hi = x.astype(BF16)
    rest = x - hi.astype(F32)
    mid = rest.astype(BF16)
    return hi, mid, (rest - mid.astype(F32)).astype(BF16)


def iota(shape, dim):
    return lax.broadcasted_iota(jnp.int32, shape, dim)


def first_head(rows):
    return iota((rows, LANES), 1) < HEAD


def stacked(x):
    own = first_head(x.shape[0])
    zero = jnp.zeros_like(x)
    return jnp.concatenate([jnp.where(own, x, zero), jnp.where(own, zero, x)], axis=0)


def folded(x):
    half = x.shape[0] // 2
    return x[:half] + x[half:]


def head_ones():
    return (iota((LANES, LANES), 0) // HEAD == iota((LANES, LANES), 1) // HEAD).astype(BF16)


def head_sum(x, ones):
    hi, lo = halves(x)
    return dg(hi, ones) + dg(lo, ones)


def sigmoid(x):
    return 1.0 / (1.0 + jnp.exp(-x))


def mixer_group(first, serve, q_ref, k_ref, v_ref, dip_ref, cri_ref, dco_ref, cro_ref, extra_ref, m_ref, n_ref, r_ref, o_ref):
    ids = range(first, first + GROUP)
    ones = head_ones()
    row, col = iota((LANES, LANES), 0), iota((LANES, LANES), 1)
    eye = (row == col).astype(F32)
    low = (iota((CH, CH), 0) >= iota((CH, CH), 1)).astype(BF16)
    ends, us, bts, avs, reads, vs = [], [], [], [], [], []
    invs, offs, qks = [], [], []
    for c in ids:
        rows = pl.ds(c * CH, CH)
        q, k, v = (r[rows, :].astype(F32) for r in (q_ref, k_ref, v_ref))
        pre = dco_ref[...] + dip_ref[rows, :].astype(F32)
        log_decay = -(sigmoid(pre) * 0.6065306597126334) - extra_ref[rows, :]
        unit = k * lax.rsqrt(head_sum(k * k, ones) + 1e-6)
        b = unit * sigmoid(cro_ref[...] + cri_ref[rows, :].astype(F32))
        total = sum(dg(low, part) for part in thirds(log_decay))
        before = total - log_decay
        mid, end = total[CH // 2 - 1 : CH // 2], total[CH - 1 :]
        up, down = jnp.exp(total - mid), jnp.exp(mid - total)
        up_before = jnp.exp(before - mid)
        rest = jnp.exp(end - total)
        left = halves(jnp.concatenate([stacked(unit * up_before), stacked(q * up)], axis=0))
        right = halves(jnp.concatenate([stacked(k * down), stacked(b * down)], axis=0))
        a = mm(left, right, 1, 1)
        a_uk = jnp.where(row > col, a[:LANES, :LANES], 0.0)
        a_qk = jnp.where(row >= col, a[LANES:, :LANES], 0.0)
        a_qb = jnp.where(row >= col, a[LANES:, LANES:], 0.0)
        offs.append(a[:LANES, LANES:])
        vst = halves(stacked(v))
        av = mm(halves(jnp.concatenate([a_uk, a_qk], axis=0)), vst)
        us.append(halves(jnp.concatenate([stacked(unit * jnp.exp(before)), av[:LANES]], axis=1)))
        avs.append(av[LANES:])
        qks.append(halves(a_qb))
        reads.append(stacked(q * jnp.exp(total)))
        bts.append(halves(stacked(b * rest)))
        ends.append((jnp.exp(end), mm(vst, halves(stacked(k * rest)), 0, 0)))
    serve(first)
    size = 1
    while size < CH:
        inside = (row // (2 * size) == col // (2 * size)) & (row // size != col // size) & (row > col)
        for i in range(GROUP):
            part = jnp.where(inside, offs[i], 0.0)
            if size == 1:
                invs.append(eye - part)
            else:
                inv = halves(invs[i])
                invs[i] = invs[i] - mm(halves(mm(inv, halves(part))), inv)
        size *= 2
    serve(first + 1)
    for i, c in enumerate(ids):
        wu = mm(halves(invs[i]), us[i])
        wu2 = halves(wu)
        ro = mm(qks[i], wu2)
        r_ref[c] = reads[i] - ro[:, :LANES]
        o_ref[c] = avs[i] - ro[:, LANES:]
        mn = mm(wu2, bts[i], 0, 0)
        decay, kv = ends[i]
        m_ref[c] = jnp.where(row == col, decay, 0.0) - mn[:LANES]
        n_ref[c] = kv - mn[LANES:]


def unpacked(message):
    wide = message.astype(F32)
    return stacked(wide[:HEAD]).astype(BF16), stacked(wide[HEAD:])


def packed(trans, state):
    return jnp.concatenate([folded(trans), folded(state)], axis=0).astype(BF16)


def after(total, message):
    trans, state = unpacked(message)
    hi, lo = halves(total)
    out = dg(hi, trans) + dg(lo, trans)
    return jnp.concatenate([out[:LANES], out[LANES:] + state], axis=0)


GQ, GP, DQ, DP = 0, 1, 2, 3
PARTS = ((0, 24, 40, True), (0, 0, 24, False), (1, 24, 40, True), (1, 0, 24, False))
Z_RINGS = (0, 2, 1, 6)
X_RINGS = (0, 16, 8, 17)
DZ = (0, -1, 1, -2, 2, -3, 3, 4)
DX = (0, 1, -1, 2)
Z_ON, Z_FIRST, X_FIRST, X_ON = 0, 1, 2, 3
SCHEDULE = {
    "start": (
        (2, 1, 0, 0), (1, 0, 0, 0), (1, 1, 0, 0), (2, 0, 0, 0),
    ),
    "a2": (
        (3, 1, 0, 0), (1, 1, 1, 0), (1, 1, 2, 0),
    ),
    "a3": (
        (2, 0, 1, 0), (0, 0, 0, 1), (2, 0, 2, 0),
    ),
    "a4": (
        (0, 1, 0, 1), (3, 0, 0, 0), (1, 1, 3, 0),
    ),
    "a5": (
        (0, 1, 1, 1),
    ),
    "xsent": (
        (0, 1, 2, 1), (3, 0, 1, 0), (2, 0, 3, 0), (2, 0, 4, 0), (0, 0, 0, 2), (3, 0, 2, 0),
    ),
    "zsent": (
        (0, 1, 3, 1), (0, 1, 0, 2), (0, 1, 1, 2), (0, 1, 2, 2), (3, 0, 3, 0), (2, 0, 5, 0),
        (2, 0, 6, 0), (0, 0, 0, 3), (3, 0, 4, 0),
    ),
    "ag1": (
        (1, 2, 0, 0), (2, 2, 0, 0), (0, 1, 3, 2), (0, 1, 0, 3), (1, 3, 0, 0), (2, 3, 0, 0),
        (3, 0, 5, 0), (0, 1, 1, 3),
    ),
    "ag2": (
        (0, 1, 2, 3), (3, 0, 6, 0),
    ),
    "ag3": (
        (2, 0, 7, 0),
    ),
    "pr0": (
        (3, 2, 0, 0), (0, 2, 0, 1), (2, 2, 1, 0), (2, 2, 2, 0),
    ),
    "pr1": (
        (1, 3, 1, 0), (1, 3, 2, 0), (3, 3, 0, 0),
    ),
    "pr2": (
        (0, 1, 3, 3),
    ),
    "gu": (
        (0, 3, 0, 1), (0, 2, 0, 2), (2, 2, 3, 0), (2, 2, 4, 0), (3, 0, 7, 0), (0, 3, 1, 1),
        (0, 3, 2, 1), (3, 2, 1, 0), (0, 3, 0, 2), (3, 2, 2, 0), (1, 3, 3, 0), (0, 2, 0, 3),
        (2, 2, 5, 0), (2, 2, 6, 0), (3, 2, 3, 0), (0, 3, 1, 2), (0, 3, 2, 2), (3, 2, 4, 0),
        (0, 3, 0, 3), (0, 3, 3, 1),
    ),
    "d0": (
        (0, 3, 1, 3), (0, 3, 2, 3), (2, 2, 7, 0),
    ),
    "d1": (
        (3, 2, 5, 0), (0, 3, 3, 2), (3, 2, 6, 0),
    ),
    "d2": (
        (0, 3, 3, 3), (3, 2, 7, 0),
    ),
}


class Gather:
    def __init__(self, bufs, send_z, recv_z, send_x, recv_x, sends):
        self.bufs, self.sends, self.here, self.done = bufs, sends, set(), set()
        self.sems = {"z": (send_z, recv_z), "x": (send_x, recv_x)}
        self.place = {"z": lax.axis_index("z"), "x": lax.axis_index("x")}

    def copy(self, axis, part, i, hop, right, got):
        buf, first, rows, z_first = PARTS[part]
        sign, far = (1 if right else -1), {"z": 4, "x": 2}[axis]
        size = {"z": NZ, "x": NX}
        back = -sign * (hop if got else hop - 1)
        dz, dx = (back, DX[i]) if axis == "z" else (DZ[i], back)
        ref = self.bufs[buf].at[lax.rem(self.place["z"] + dz + NZ, NZ), lax.rem(self.place["x"] + dx + NX, NX)]
        if hop == far:
            cut = (rows // 8 + i % 2) // 2 * 8
            first, rows = (first, cut) if right else (first + cut, rows - cut)
        ref = ref.at[pl.ds(first, rows)]
        ring = (Z_RINGS if axis == "z" else X_RINGS)[part] + i
        slot = hop - 1 + (0 if right else far)
        send, recv = self.sems[axis]
        return pltpu.make_async_remote_copy(
            ref, ref, send.at[ring, slot], recv.at[ring, slot],
            device_id={axis: lax.rem(self.place[axis] + sign + size[axis], size[axis])}, device_id_type=MESH,
        )

    def send(self, axis, part, i, hop):
        for right in (True, False):
            copy = self.copy(axis, part, i, hop, right, False)
            copy.start()
            self.sends.append(copy)

    def need(self, axis, part, i, hop):
        if (axis, part, i, hop) not in self.here:
            self.here.add((axis, part, i, hop))
            for right in (True, False):
                self.copy(axis, part, i, hop, right, True).wait_recv()

    def do(self, kind, part, i, hop):
        self.done.add((kind, part, i, hop))
        z_first = PARTS[part][3]
        if kind == Z_ON:
            self.need("z", part, i, hop)
            self.send("z", part, i, hop + 1)
        elif kind == Z_FIRST:
            if not z_first and i:
                self.need("x", part, 0, 1 if i < 3 else 2)
            self.send("z", part, i, 1)
        elif kind == X_FIRST:
            if z_first and i:
                self.need("z", part, 0, (i + 1) // 2)
            self.send("x", part, i, 1)
        else:
            self.need("x", part, i, 1)
            self.send("x", part, i, 2)

    def serve(self, point):
        for task in SCHEDULE.get(point, ()):
            self.do(*task)

    def whole(self, part):
        for i in range(8 if PARTS[part][3] else 1):
            self.need("x", part, i, 1)
            self.need("x", part, i, 2)
        for i in range(1 if PARTS[part][3] else 4):
            for hop in range(1, 5):
                self.need("z", part, i, hop)

    def slab(self, q, p, i):
        hop = (i + 1) // 2
        if i:
            self.need("z", q, 0, hop)
            for j in range(4):
                self.need("z", p, j, hop)
        for part, ring in ((q, i), (p, 0)):
            self.need("x", part, ring, 1)
            self.need("x", part, ring, 2)


class Spread:
    def __init__(self, block, send_sem, recv_sem, sends):
        self.block, self.send_sem, self.recv_sem, self.sends = block, send_sem, recv_sem, sends
        self.y, self.c = lax.axis_index("y"), lax.axis_index("c")

    def along_y(self, sem, dy, up, half):
        ref = self.block(lax.rem(self.y + dy + NY, NY) * NC + self.c, half)
        return pltpu.make_async_remote_copy(
            ref, ref, self.send_sem.at[sem], self.recv_sem.at[sem],
            device_id={"y": lax.rem(self.y + (1 if up else NY - 1), NY)}, device_id_type=MESH,
        )

    def across(self, sem, dy, mine):
        ref = self.block(lax.rem(self.y + dy + NY, NY) * NC + (self.c if mine else 1 - self.c), None)
        return pltpu.make_async_remote_copy(
            ref, ref, self.send_sem.at[sem], self.recv_sem.at[sem], device_id={"c": 1 - self.c}, device_id_type=MESH
        )

    def go(self, copy):
        copy.start()
        self.sends.append(copy)

    def start(self):
        for half in (0, 1):
            self.go(self.along_y(half, 0, True, half))
            self.go(self.along_y(2 + half, 0, False, 1 - half))
        self.go(self.across(6, 0, True))

    def relay(self):
        self.along_y(0, -1, True, 0).wait_recv()
        self.go(self.along_y(4, -1, True, 0))
        self.along_y(2, 1, False, 1).wait_recv()
        self.go(self.along_y(5, 1, False, 1))

    def near(self):
        self.along_y(1, -1, True, 1).wait_recv()
        self.go(self.across(7, -1, True))
        self.along_y(3, 1, False, 0).wait_recv()
        self.go(self.across(8, 1, True))

    def far(self):
        self.along_y(4, 2, True, 0).wait_recv()
        self.along_y(5, 2, False, 1).wait_recv()
        self.go(self.across(9, 2, True))

    def finish(self):
        for sem, dy in ((6, 0), (7, -1), (8, 1), (9, 2)):
            self.across(sem, dy, False).wait_recv()


_open = []


def mark(name):
    if _open:
        _open.pop().__exit__(None, None, None)
    if name:
        _open.append(jax.named_scope(name))
        _open[-1].__enter__()


def kernel(
    q_hbm, k_hbm, v_hbm, dip_hbm, cri_hbm, dco_hbm, cro_hbm, gain_hbm, extra_t_hbm, fng_hbm,
    resid_hbm, wo_hbm, gate_hbm, up_hbm, down_hbm,
    out_ref,
    q_ref, k_ref, v_ref, dip_ref, cri_ref, dco_ref, cro_ref, gain_ref, extra_t_ref, fng_ref,
    wgu, wd, g_in, u_in, wo, resid,
    extra_ref, m_ref, n_ref, r_ref, o_ref, gm_ref, hm_ref,
    tot_ref, xbuf, xpre, zsrc, zbuf, s_ref,
    mix_all, mid_ref, rows, hid_ref,
    full_part, own_part, pair, sib_src, sib_buf, far_src, far_buf, y_src, y_buf,
    local_sem, send_z, recv_z, send_x, recv_x,
    st_send, st_recv, res_send, res_recv, ag_send, ag_recv, rs_send, rs_recv,
):
    z, x, y, c = (lax.axis_index(n) for n in SP_TP)
    tp = y * NC + c
    sends = []
    tokens, width = rows.shape
    share = tokens // NT

    def block_rows(i):
        return pl.ds(pl.multiple_of(i * share, 16), share)

    def go(copy):
        copy.start()
        sends.append(copy)

    mark("barrier")
    own = [
        pltpu.make_async_copy(src, dst, local_sem.at[i])
        for i, (src, dst) in enumerate(
            ((gate_hbm, g_in), (up_hbm, u_in), (down_hbm, wd.at[z, x]), (resid_hbm, resid.at[block_rows(tp)]),
             (extra_t_hbm, extra_t_ref), (k_hbm, k_ref), (q_hbm, q_ref), (v_hbm, v_ref), (dip_hbm, dip_ref),
             (cri_hbm, cri_ref), (dco_hbm, dco_ref), (cro_hbm, cro_ref), (gain_hbm, gain_ref), (fng_hbm, fng_ref), (wo_hbm, wo))
        )
    ]
    barrier = pltpu.get_barrier_semaphore()
    peers = [{"x": lax.rem(x + d, NX)} for d in range(1, NX)]
    peers += [{"z": lax.rem(z + d, NZ)} for d in range(1, NZ)]
    peers += [{"y": lax.rem(y + d, NY)} for d in (1, NY - 1)] + [{"c": 1 - c}]
    for peer in peers:
        pl.semaphore_signal(barrier, inc=1, device_id=peer, device_id_type=MESH)
    for copy in own:
        copy.start()
    for copy in own[:5]:
        copy.wait()
    hidden = g_in.shape[1]
    full = hidden // LANES * LANES
    wgu[z, x, :, :full] = g_in[:, :full]
    wgu[z, x, :, full : 2 * full] = u_in[:, :full]
    tail = jnp.concatenate([g_in[:, full:].astype(F32), u_in[:, full:].astype(F32)], axis=1)
    wgu[z, x, :, 2 * full :] = tail.astype(BF16)
    extra_t = jnp.concatenate([extra_t_ref[...], jnp.zeros((6, extra_t_ref.shape[1]), F32)], axis=0)
    pick = (iota((8, LANES), 0) == iota((8, LANES), 1) // HEAD).astype(BF16)
    extra_ref[...] = sum(dg(part, pick, 0, 0) for part in thirds(extra_t))
    pl.semaphore_wait(barrier, len(peers))

    g = Gather((wgu, wd), send_z, recv_z, send_x, recv_x, sends)
    g.serve("start")

    def resid_block(i, half):
        cols = pl.ds(0, width) if half is None else pl.ds(half * (width // 2), width // 2)
        return resid.at[block_rows(i), cols]

    def mix_block(i, half):
        part = pl.ds(0, tokens) if half is None else pl.ds(half * (tokens // 2), tokens // 2)
        return mix_all.at[part, pl.ds(pl.multiple_of(i * LANES, LANES), LANES)]

    res = Spread(resid_block, res_send, res_recv, sends)
    res.start()

    mix = functools.partial(
        mixer_group, serve=lambda i: g.serve(f"a{i}"), q_ref=q_ref, k_ref=k_ref, v_ref=v_ref, dip_ref=dip_ref, cri_ref=cri_ref, dco_ref=dco_ref,
        cro_ref=cro_ref, extra_ref=extra_ref, m_ref=m_ref, n_ref=n_ref, r_ref=r_ref, o_ref=o_ref,
    )
    for copy in own[5:14]:
        copy.wait()
    mark("mix0")
    mix(0)
    mark("s1")
    g.serve("a2")
    res.relay()
    mark("mix1")
    mix(GROUP)
    mark("s2")
    g.serve("a5")
    res.near()
    res.far()
    mark("prefix")

    row, col = iota((LANES, LANES), 0), iota((LANES, LANES), 1)
    start = jnp.concatenate([(row == col).astype(F32), jnp.zeros((LANES, LANES), F32)], axis=0)
    total = start
    for i in range(CHUNKS):
        split = halves(total)
        step = mm(split, halves(m_ref[i]))
        gh = mm(halves(r_ref[i]), split, 1, 1)
        rows_i = pl.ds(i * CH, CH)
        gm_ref[rows_i, :] = folded(gh[:, :LANES])
        hm_ref[rows_i, :] = folded(gh[:, LANES:] + o_ref[i])
        total = jnp.concatenate([step[:LANES], step[LANES:] + n_ref[i]], axis=0)
    tot_ref[...] = packed(total[:LANES], total[LANES:])

    def x_state(d):
        return pltpu.make_async_remote_copy(
            tot_ref, xbuf.at[d - 1], st_send.at[d - 1], st_recv.at[d - 1],
            device_id={"x": lax.rem(x + d, NX)}, device_id_type=MESH,
        )

    for d in range(1, NX):
        go(x_state(d))
    mark("s2")
    g.serve("xsent")
    mark("xstate")
    for d in range(1, NX):
        x_state(d).wait_recv()
    mark("xcomb")
    total = start
    prefix = total
    for i in range(NX):
        prefix = jnp.where(x == i, total, prefix)
        message = tot_ref[...]
        for d in range(1, NX):
            message = jnp.where(lax.rem(x - i + NX, NX) == d, xbuf[d - 1], message)
        total = after(total, message)
    xpre[...] = prefix
    zsrc[...] = packed(total[:LANES], total[LANES:])

    def z_state(d):
        return pltpu.make_async_remote_copy(
            zsrc, zbuf.at[d - 1], st_send.at[NX - 2 + d], st_recv.at[NX - 2 + d],
            device_id={"z": lax.rem(z + d, NZ)}, device_id_type=MESH,
        )

    for d in range(1, NZ):
        pl.when(z + d < NZ)(lambda d=d: z_state(d).start())
    mark("s3")
    g.serve("zsent")
    mark("zstate")
    s_ref[...] = jnp.zeros_like(s_ref)
    for d in range(NZ - 1, 0, -1):

        @pl.when(z >= d)
        def _(d=d):
            z_state(d).wait_recv()
            trans, state = unpacked(zbuf[d - 1])
            hi, lo = halves(s_ref[...])
            s_ref[...] = dg(hi, trans) + dg(lo, trans) + state

    mark("read")
    incoming = mm(halves(s_ref[...]), halves(xpre[:LANES])) + xpre[LANES:]
    read = mm(halves(gm_ref[...]), halves(incoming), 1, 1) + hm_ref[...]
    ones = head_ones()
    center = read - head_sum(read, ones) * (1.0 / HEAD)
    spread = head_sum(center * center, ones) * (1.0 / HEAD)
    mine = pl.ds(pl.multiple_of(tp * LANES, LANES), LANES)
    mix_all[:, mine] = (center * lax.rsqrt(spread + 1e-5) * gain_ref[...]).astype(BF16)
    mixed = Spread(mix_block, ag_send, ag_recv, sends)
    mixed.start()
    mark("ag1")
    g.serve("ag1")
    mark("ag1w")
    mixed.relay()
    mark("ag2")
    g.serve("ag2")
    mark("ag2w")
    mixed.near()
    mixed.far()
    mark("ag3")
    g.serve("ag3")
    mark("ag3w")
    own[14].wait()
    res.finish()
    mixed.finish()

    tile = 512
    square = jnp.zeros((tokens, 1), F32)
    for i in range(width // tile):
        mark(f"pr{i}")
        cols = pl.ds(i * tile, tile)
        proj = jnp.dot(mix_all[...], wo[:, cols], preferred_element_type=F32)
        mid = (resid[:, cols].astype(F32) + proj).astype(BF16)
        mid_ref[:, cols] = mid
        mid = mid.astype(F32)
        square += jnp.sum(mid * mid, axis=-1, keepdims=True)
        mark(f"sp{i}")
        g.serve(f"pr{i}")
    mark("norm")
    scale = lax.rsqrt(square * (1.0 / width) + 1e-6)
    for i in range(width // tile):
        cols = pl.ds(i * tile, tile)
        rows[:, cols] = (mid_ref[:, cols].astype(F32) * scale * fng_ref[:, cols]).astype(BF16)
    mark("gu")
    g.serve("gu")
    g.whole(GQ)
    g.whole(GP)

    mark("gateup")
    both = jnp.dot(rows[...], wgu[...].reshape(width, 2 * hidden), preferred_element_type=F32)

    def gated(gate, upper):
        return (gate * sigmoid(gate) * upper).astype(BF16)

    rest = hidden - full
    hid_ref[:, :full] = gated(both[:, :full], both[:, full : 2 * full])
    hid_ref[:, full:] = gated(both[:, 2 * full : 2 * full + rest], both[:, 2 * full + rest :])

    slab = width // NZ

    def wide(n):
        return len(COLS[n]) * slab

    def to_mate(n):
        cols = pl.ds(0, wide(n))
        return pltpu.make_async_remote_copy(
            sib_src.at[n, :, :, cols], sib_buf.at[n, :, :, cols], rs_send.at[n, 0], rs_recv.at[n, 0],
            device_id={"c": 1 - c}, device_id_type=MESH,
        )

    def to_y(n, kind, up):
        src, dst = (far_src, far_buf) if kind == 0 else (y_src, y_buf)
        cols = pl.ds(0, wide(n) // 2 if kind == 0 else wide(n))
        k = 0 if up else 1
        sem = 1 + 2 * kind + k
        return pltpu.make_async_remote_copy(
            src.at[n, k, :, cols], dst.at[n, k, :, cols], rs_send.at[n, sem], rs_recv.at[n, sem],
            device_id={"y": lax.rem(y + (1 if up else NY - 1), NY)}, device_id_type=MESH,
        )

    def place(i):
        return lax.rem(z + DZ[i] + NZ, NZ)

    def product(n):
        for k, i in enumerate(COLS[n]):
            full_part[n, :, k * slab : (k + 1) * slab] = dg(hid_ref[...], wd[place(i)].reshape(slab, hidden), 1, 1)
        for yy in range(NY):
            sib_src[n, yy, :, : wide(n)] = full_part[n, block_rows(yy * NC + 1 - c), : wide(n)].astype(BF16)
        go(to_mate(n))

    def chip_sum(n):
        to_mate(n).wait_recv()
        w, h = wide(n), wide(n) // 2

        def of(d):
            yy = lax.rem(y + d, NY)
            return full_part[n, block_rows(yy * NC + c), :w] + sib_buf[n, yy, :, :w].astype(F32)

        far = of(2).astype(BF16)
        far_src[n, 0, :, :h] = far[:, :h]
        far_src[n, 1, :, :h] = far[:, h:]
        go(to_y(n, 0, True))
        go(to_y(n, 0, False))
        own_part[n, :, :w] = of(0)
        pair[n, 0, :, :w] = of(1)
        pair[n, 1, :, :w] = of(3)

    def ring_sum(n):
        w, h = wide(n), wide(n) // 2
        to_y(n, 0, True).wait_recv()
        y_src[n, 0, :, :h] = (pair[n, 0, :, :h] + far_buf[n, 0, :, :h].astype(F32)).astype(BF16)
        y_src[n, 0, :, h:w] = pair[n, 0, :, h:w].astype(BF16)
        go(to_y(n, 1, True))
        to_y(n, 0, False).wait_recv()
        y_src[n, 1, :, :h] = pair[n, 1, :, :h].astype(BF16)
        y_src[n, 1, :, h:w] = (pair[n, 1, :, h:w] + far_buf[n, 1, :, :h].astype(F32)).astype(BF16)
        go(to_y(n, 1, False))

    def finish(n):
        for up in (True, False):
            to_y(n, 1, up).wait_recv()
        for k, i in enumerate(COLS[n]):
            at = slice(k * slab, (k + 1) * slab)
            acc = own_part[n, :, at] + y_buf[n, 0, :, at].astype(F32) + y_buf[n, 1, :, at].astype(F32)
            cols = pl.ds(pl.multiple_of(place(i) * slab, slab), slab)
            out_ref[:, cols] = (mid_ref[block_rows(tp), cols].astype(F32) + 0.5 * acc).astype(BF16)

    for n in range(len(COLS)):
        mark(f"d{n}")
        g.serve(f"d{n}")
        if n > 0:
            chip_sum(n - 1)
        if n > 1:
            ring_sum(n - 2)
        mark(f"w{n}")
        for i in COLS[n]:
            g.slab(DQ, DP, i)
        mark(f"p{n}")
        product(n)
    last = len(COLS) - 1
    mark("cs3")
    chip_sum(last)
    mark("rs2")
    ring_sum(last - 1)
    mark("fin01")
    for n in range(last - 1):
        finish(n)
    mark("rs3")
    ring_sum(last)
    mark("fin2")
    finish(last - 1)
    mark("fin3")
    finish(last)
    mark("sendwait")
    for copy in sends:
        copy.wait_send()
    for d in range(1, NZ):
        pl.when(z + d < NZ)(lambda d=d: z_state(d).wait_send())
    mark(None)


def per_device(
    resid, queries, keys, values, decay_input_part, decay_channel_offset, decay_head_extra, correction_rate_input,
    correction_rate_offset, head_norm_gain, mixer_output_weight, feedforward_norm_gain, gate_weight, up_weight, down_weight,
):
    tokens = queries.shape[0]
    share, width = resid.shape
    shard, hidden = gate_weight.shape
    vm, sem = pltpu.VMEM, pltpu.SemaphoreType.DMA
    flat = pl.BlockSpec(memory_space=pltpu.VMEM)
    there = pl.BlockSpec(memory_space=pl.ANY)
    slab = width // NZ
    parts, wide = len(COLS), max(map(len, COLS)) * slab
    return pl.pallas_call(
        kernel,
        name="layer",
        out_shape=pltpu.VMEM((share, width), BF16),
        in_specs=[there] * 15,
        out_specs=flat,
        scratch_shapes=[
            *[vm((tokens, LANES), BF16)] * 5, *[vm((1, LANES), F32)] * 3, vm((LANES // HEAD, tokens), F32), vm((1, width), F32),
            vm((NZ, NX, shard, 2 * hidden), BF16), vm((NZ, NX, shard, hidden), BF16),
            vm((shard, hidden), BF16), vm((shard, hidden), BF16),
            vm(mixer_output_weight.shape, BF16), vm((tokens, width), BF16),
            vm((tokens, LANES), F32),
            vm((CHUNKS, LANES, LANES), F32), vm((CHUNKS, LANES, LANES), F32),
            vm((CHUNKS, LANES, LANES), F32), vm((CHUNKS, LANES, LANES), F32),
            vm((tokens, LANES), F32), vm((tokens, LANES), F32),
            vm((LANES, LANES), BF16), vm((NX - 1, LANES, LANES), BF16), vm((2 * LANES, LANES), F32),
            vm((LANES, LANES), BF16), vm((NZ - 1, LANES, LANES), BF16), vm((LANES, LANES), F32),
            vm((tokens, NT * LANES), BF16), vm((tokens, width), BF16), vm((tokens, width), BF16), vm((tokens, hidden), BF16),
            vm((parts, tokens, wide), F32), vm((parts, share, wide), F32), vm((parts, 2, share, wide), F32),
            vm((parts, NY, share, wide), BF16), vm((parts, NY, share, wide), BF16),
            vm((parts, 2, share, wide // 2), BF16), vm((parts, 2, share, wide // 2), BF16),
            vm((parts, 2, share, wide), BF16), vm((parts, 2, share, wide), BF16),
            sem((15,)), sem((10, 8)), sem((10, 8)), sem((18, 4)), sem((18, 4)),
            sem((NX + NZ - 2,)), sem((NX + NZ - 2,)), sem((10,)), sem((10,)), sem((10,)), sem((10,)),
            sem((parts, 5)), sem((parts, 5)),
        ],
        compiler_params=pltpu.CompilerParams(collective_id=0, has_side_effects=True),
    )(
        queries, keys, values, decay_input_part, correction_rate_input,
        decay_channel_offset[None], correction_rate_offset[None], head_norm_gain[None], decay_head_extra.T,
        feedforward_norm_gain[None], resid, mixer_output_weight, gate_weight, up_weight, down_weight.T,
    )


def solution(mesh):
    torus = Mesh(mesh.devices.reshape(NZ, NX, NY, NC), SP_TP)
    in_specs = (
        P(SP_TP, None), P(SP, TP), P(SP, TP), P(SP, TP), P(SP, TP), P(TP), P(SP, TP), P(SP, TP), P(TP), P(TP),
        P(), P(), P(SP, TP), P(SP, TP), P(TP, SP),
    )
    return jax.shard_map(per_device, mesh=torus, in_specs=in_specs, out_specs=P(SP_TP, None), check_vma=False)
```

time: 108 us -> 83 us (0.77)
  Pallas kernels: 105 us -> 82.2 us
  local copies, waits for them, and re-layouts: 3.12 us -> 0.68 us
    pallas_call x1, Pallas kernels: 105 us -> 82.2 us  [per_device(): pl.pallas_call(kernel, name='layer', out_shape=pltpu.VMEM((share, width),...]
where the time goes in v2:
time: 83 us; the launch traced here: 82.9 us
  Pallas kernels  82.2 us (99%)
    pallas_call x1, Pallas kernels, per_device(): pl.pallas_call(kernel, name='layer', out_shape=pltpu.VMEM((share, width),...  82.2 us

profile of v2, /device:TPU:1, one launch (start us, length us, event | category | flops | bytes accessed | tf_op | source)
XLA Modules:
  0.0 82.9 jit_solution(3108526745557865784)
XLA Ops:
  0.0 82.2 %layer.1 = bf16[48,2048]{1,0:T(8,128)(2,1)S(1)} custom-call(bf16[384,128]{1,0:T(8,128)(2,1)} %q_hbm.1, bf16[384,128]{1,0:T(8,128)(2,1)} %k_hbm.1, bf16[384,128]{1,0:T(8,128)(2,1)} %v_hbm.1, bf16[384,128]{1,0:T(8,128)(2,1)} %dip_hbm.1, bf16[384,128]{1,0:T(8,128)(2,1)} %cri_hbm.1, f32[1,128]{1,0:T(1,128)} %bitcast.9, f32[1,128]{1,0:T(1,128)} %bitcast.10, ...), custom_call_target="tpu_custom_call" | custom-call | tf_op jit(solution)/shard_map/layer/pallas_call | solution.py:678
  82.2 0.7 copy.17

commit v3 on v2

--- a/solution.py
+++ b/solution.py
@@ -13,6 +13,7 @@
 HEAD, LANES, CH = 64, 128, 64
 NZ, NX, NY, NC = 8, 4, 4, 2
 NT = NY * NC
+ZG = NZ // 2
 CHUNKS = 6
 GROUP = 3
 COLS = ((0, 1, 2), (3, 4), (5, 6), (7,))
@@ -149,7 +150,7 @@
 
 
 GQ, GP, DQ, DP = 0, 1, 2, 3
-PARTS = ((0, 24, 40, True), (0, 0, 24, False), (1, 24, 40, True), (1, 0, 24, False))
+PARTS = ((0, 24, 40, True), (0, 0, 24, False), (1, 32, 32, True), (1, 0, 32, False))
 Z_RINGS = (0, 2, 1, 6)
 X_RINGS = (0, 16, 8, 17)
 DZ = (0, -1, 1, -2, 2, -3, 3, 4)
@@ -157,60 +158,62 @@
 Z_ON, Z_FIRST, X_FIRST, X_ON = 0, 1, 2, 3
 SCHEDULE = {
     "start": (
-        (2, 1, 0, 0), (1, 0, 0, 0), (1, 1, 0, 0), (2, 0, 0, 0),
+        (1, 2, 0, 0), (1, 3, 0, 0), (2, 1, 0, 0), (2, 3, 0, 0), (1, 0, 0, 0), (1, 1, 0, 0),
+        (2, 0, 0, 0),
+    ),
+    "a1": (
+        (2, 2, 0, 0),
     ),
     "a2": (
-        (3, 1, 0, 0), (1, 1, 1, 0), (1, 1, 2, 0),
+        (0, 2, 0, 1), (1, 1, 1, 0), (3, 1, 0, 0), (1, 1, 2, 0), (2, 2, 1, 0),
     ),
     "a3": (
-        (2, 0, 1, 0), (0, 0, 0, 1), (2, 0, 2, 0),
+        (3, 3, 0, 0), (0, 0, 0, 1), (2, 0, 1, 0),
     ),
     "a4": (
-        (0, 1, 0, 1), (3, 0, 0, 0), (1, 1, 3, 0),
-    ),
-    "a5": (
-        (0, 1, 1, 1),
+        (0, 1, 0, 1),
     ),
     "xsent": (
-        (0, 1, 2, 1), (3, 0, 1, 0), (2, 0, 3, 0), (2, 0, 4, 0), (0, 0, 0, 2), (3, 0, 2, 0),
+        (3, 0, 0, 0), (1, 1, 3, 0), (2, 0, 2, 0), (0, 1, 1, 1), (3, 0, 1, 0), (2, 0, 3, 0),
+        (2, 0, 4, 0),
     ),
     "zsent": (
-        (0, 1, 3, 1), (0, 1, 0, 2), (0, 1, 1, 2), (0, 1, 2, 2), (3, 0, 3, 0), (2, 0, 5, 0),
-        (2, 0, 6, 0), (0, 0, 0, 3), (3, 0, 4, 0),
+        (0, 0, 0, 2), (0, 1, 2, 1), (0, 1, 0, 2), (3, 0, 2, 0), (2, 2, 2, 0),
+    ),
+    "z2sent": (
+        (3, 0, 3, 0), (1, 3, 1, 0), (0, 0, 0, 3), (2, 0, 5, 0), (2, 0, 6, 0), (0, 1, 3, 1),
+        (0, 1, 1, 2), (0, 1, 2, 2), (3, 0, 4, 0), (0, 1, 0, 3),
     ),
     "ag1": (
-        (1, 2, 0, 0), (2, 2, 0, 0), (0, 1, 3, 2), (0, 1, 0, 3), (1, 3, 0, 0), (2, 3, 0, 0),
-        (3, 0, 5, 0), (0, 1, 1, 3),
+        (2, 0, 7, 0), (1, 3, 2, 0), (3, 0, 5, 0), (0, 1, 3, 2), (0, 1, 1, 3),
     ),
     "ag2": (
-        (0, 1, 2, 3), (3, 0, 6, 0),
+        (3, 0, 6, 0), (1, 3, 3, 0), (0, 1, 2, 3), (2, 2, 3, 0), (0, 2, 0, 2),
     ),
     "ag3": (
-        (2, 0, 7, 0),
+        (3, 2, 0, 0), (0, 3, 0, 1), (2, 2, 4, 0),
     ),
     "pr0": (
-        (3, 2, 0, 0), (0, 2, 0, 1), (2, 2, 1, 0), (2, 2, 2, 0),
-    ),
-    "pr1": (
-        (1, 3, 1, 0), (1, 3, 2, 0), (3, 3, 0, 0),
+        (3, 0, 7, 0), (0, 3, 1, 1), (0, 1, 3, 3),
     ),
     "pr2": (
-        (0, 1, 3, 3),
+        (0, 3, 2, 1), (3, 2, 1, 0),
+    ),
+    "pr3": (
+        (3, 2, 2, 0), (0, 3, 3, 1),
     ),
     "gu": (
-        (0, 3, 0, 1), (0, 2, 0, 2), (2, 2, 3, 0), (2, 2, 4, 0), (3, 0, 7, 0), (0, 3, 1, 1),
-        (0, 3, 2, 1), (3, 2, 1, 0), (0, 3, 0, 2), (3, 2, 2, 0), (1, 3, 3, 0), (0, 2, 0, 3),
-        (2, 2, 5, 0), (2, 2, 6, 0), (3, 2, 3, 0), (0, 3, 1, 2), (0, 3, 2, 2), (3, 2, 4, 0),
-        (0, 3, 0, 3), (0, 3, 3, 1),
+        (2, 2, 5, 0), (3, 2, 3, 0), (0, 2, 0, 3), (2, 2, 6, 0), (0, 3, 0, 2), (3, 2, 4, 0),
+        (0, 3, 1, 2),
     ),
     "d0": (
-        (0, 3, 1, 3), (0, 3, 2, 3), (2, 2, 7, 0),
+        (0, 3, 2, 2), (0, 3, 3, 2), (3, 2, 5, 0), (2, 2, 7, 0),
     ),
     "d1": (
-        (3, 2, 5, 0), (0, 3, 3, 2), (3, 2, 6, 0),
+        (3, 2, 6, 0), (0, 3, 0, 3), (0, 3, 1, 3),
     ),
     "d2": (
-        (0, 3, 3, 3), (3, 2, 7, 0),
+        (0, 3, 2, 3), (3, 2, 7, 0), (0, 3, 3, 3),
     ),
 }
 
@@ -361,7 +364,7 @@
     q_ref, k_ref, v_ref, dip_ref, cri_ref, dco_ref, cro_ref, gain_ref, extra_t_ref, fng_ref,
     wgu, wd, g_in, u_in, wo, resid,
     extra_ref, m_ref, n_ref, r_ref, o_ref, gm_ref, hm_ref,
-    tot_ref, xbuf, xpre, zsrc, zbuf, s_ref,
+    tot_ref, xbuf, xpre, zsrc, zbuf, s_ref, z2src, z2buf,
     mix_all, mid_ref, rows, hid_ref,
     full_part, own_part, pair, sib_src, sib_buf, far_src, far_buf, y_src, y_buf,
     local_sem, send_z, recv_z, send_x, recv_x,
@@ -481,29 +484,50 @@
     xpre[...] = prefix
     zsrc[...] = packed(total[:LANES], total[LANES:])
 
+    place_z, far_half = lax.rem(z, ZG), z >= ZG
+
     def z_state(d):
         return pltpu.make_async_remote_copy(
             zsrc, zbuf.at[d - 1], st_send.at[NX - 2 + d], st_recv.at[NX - 2 + d],
             device_id={"z": lax.rem(z + d, NZ)}, device_id_type=MESH,
         )
 
-    for d in range(1, NZ):
-        pl.when(z + d < NZ)(lambda d=d: z_state(d).start())
+    def z_half(d):
+        return pltpu.make_async_remote_copy(
+            z2src, z2buf, st_send.at[NX + ZG - 3 + d], st_recv.at[NX + ZG - 2],
+            device_id={"z": lax.rem(z + d, NZ)}, device_id_type=MESH,
+        )
+
+    for d in range(1, ZG):
+        pl.when(place_z + d < ZG)(lambda d=d: z_state(d).start())
     mark("s3")
     g.serve("zsent")
     mark("zstate")
-    s_ref[...] = jnp.zeros_like(s_ref)
-    for d in range(NZ - 1, 0, -1):
-
-        @pl.when(z >= d)
+    s_ref[...] = start
+    for d in range(ZG - 1, 0, -1):
+
+        @pl.when(place_z >= d)
         def _(d=d):
             z_state(d).wait_recv()
-            trans, state = unpacked(zbuf[d - 1])
-            hi, lo = halves(s_ref[...])
-            s_ref[...] = dg(hi, trans) + dg(lo, trans) + state
+            s_ref[...] = after(s_ref[...], zbuf[d - 1])
+
+    @pl.when(z == ZG - 1)
+    def _():
+        z2src[...] = folded(after(s_ref[...], zsrc[...])[LANES:]).astype(BF16)
+        for d in range(1, ZG + 1):
+            z_half(d).start()
+
+    mark("s3b")
+    g.serve("z2sent")
+    mark("zhalf")
+
+    @pl.when(far_half)
+    def _():
+        z_half(1).wait_recv()
+        s_ref[LANES:] += mm(halves(stacked(z2buf[...].astype(F32))), halves(s_ref[:LANES]))
 
     mark("read")
-    incoming = mm(halves(s_ref[...]), halves(xpre[:LANES])) + xpre[LANES:]
+    incoming = mm(halves(s_ref[LANES:]), halves(xpre[:LANES])) + xpre[LANES:]
     read = mm(halves(gm_ref[...]), halves(incoming), 1, 1) + hm_ref[...]
     ones = head_ones()
     center = read - head_sum(read, ones) * (1.0 / HEAD)
@@ -658,8 +682,14 @@
     mark("sendwait")
     for copy in sends:
         copy.wait_send()
-    for d in range(1, NZ):
-        pl.when(z + d < NZ)(lambda d=d: z_state(d).wait_send())
+    for d in range(1, ZG):
+        pl.when(place_z + d < ZG)(lambda d=d: z_state(d).wait_send())
+
+    @pl.when(z == ZG - 1)
+    def _():
+        for d in range(1, ZG + 1):
+            z_half(d).wait_send()
+
     mark(None)
 
 
@@ -691,14 +721,15 @@
             vm((CHUNKS, LANES, LANES), F32), vm((CHUNKS, LANES, LANES), F32),
             vm((tokens, LANES), F32), vm((tokens, LANES), F32),
             vm((LANES, LANES), BF16), vm((NX - 1, LANES, LANES), BF16), vm((2 * LANES, LANES), F32),
-            vm((LANES, LANES), BF16), vm((NZ - 1, LANES, LANES), BF16), vm((LANES, LANES), F32),
+            vm((LANES, LANES), BF16), vm((ZG - 1, LANES, LANES), BF16), vm((2 * LANES, LANES), F32),
+            vm((HEAD, LANES), BF16), vm((HEAD, LANES), BF16),
             vm((tokens, NT * LANES), BF16), vm((tokens, width), BF16), vm((tokens, width), BF16), vm((tokens, hidden), BF16),
             vm((parts, tokens, wide), F32), vm((parts, share, wide), F32), vm((parts, 2, share, wide), F32),
             vm((parts, NY, share, wide), BF16), vm((parts, NY, share, wide), BF16),
             vm((parts, 2, share, wide // 2), BF16), vm((parts, 2, share, wide // 2), BF16),
             vm((parts, 2, share, wide), BF16), vm((parts, 2, share, wide), BF16),
             sem((15,)), sem((10, 8)), sem((10, 8)), sem((18, 4)), sem((18, 4)),
-            sem((NX + NZ - 2,)), sem((NX + NZ - 2,)), sem((10,)), sem((10,)), sem((10,)), sem((10,)),
+            sem((NX + 2 * ZG - 2,)), sem((NX + ZG - 1,)), sem((10,)), sem((10,)), sem((10,)), sem((10,)),
             sem((parts, 5)), sem((parts, 5)),
         ],
         compiler_params=pltpu.CompilerParams(collective_id=0, has_side_effects=True),

time: 83 us -> 75.4 us (0.908)
  Pallas kernels: 82.2 us -> 74.7 us
    pallas_call x1, Pallas kernels: 82.2 us -> 74.7 us  [per_device(): pl.pallas_call(kernel, name='layer', out_shape=pltpu.VMEM((share, width),...]
where the time goes in v3:
time: 75.4 us
  Pallas kernels  74.7 us (99%)
    pallas_call x1, Pallas kernels, per_device(): pl.pallas_call(kernel, name='layer', out_shape=pltpu.VMEM((share, width),...  74.7 us

profile of v3, /device:TPU:1, one launch (start us, length us, event | category | flops | bytes accessed | tf_op | source)
XLA Modules:
  0.0 75.4 jit_solution(6563598986160694328)
XLA Ops:
  0.0 74.7 %layer.1 = bf16[48,2048]{1,0:T(8,128)(2,1)S(1)} custom-call(bf16[384,128]{1,0:T(8,128)(2,1)} %q_hbm.1, bf16[384,128]{1,0:T(8,128)(2,1)} %k_hbm.1, bf16[384,128]{1,0:T(8,128)(2,1)} %v_hbm.1, bf16[384,128]{1,0:T(8,128)(2,1)} %dip_hbm.1, bf16[384,128]{1,0:T(8,128)(2,1)} %cri_hbm.1, f32[1,128]{1,0:T(1,128)} %bitcast.9, f32[1,128]{1,0:T(1,128)} %bitcast.10, ...), custom_call_target="tpu_custom_call" | custom-call | tf_op jit(solution)/shard_map/layer/pallas_call | solution.py:708
  74.7 0.7 copy.17

commit v4 on v3

--- a/solution.py
+++ b/solution.py
@@ -150,7 +150,7 @@
 
 
 GQ, GP, DQ, DP = 0, 1, 2, 3
-PARTS = ((0, 24, 40, True), (0, 0, 24, False), (1, 32, 32, True), (1, 0, 32, False))
+PARTS = ((0, 24, 40, True), (0, 0, 24, False), (1, 16, 16, True), (1, 0, 16, False))
 Z_RINGS = (0, 2, 1, 6)
 X_RINGS = (0, 16, 8, 17)
 DZ = (0, -1, 1, -2, 2, -3, 3, 4)
@@ -158,59 +158,65 @@
 Z_ON, Z_FIRST, X_FIRST, X_ON = 0, 1, 2, 3
 SCHEDULE = {
     "start": (
-        (1, 2, 0, 0), (1, 3, 0, 0), (2, 1, 0, 0), (2, 3, 0, 0), (1, 0, 0, 0), (1, 1, 0, 0),
-        (2, 0, 0, 0),
+        (2, 0, 0, 0), (2, 1, 0, 0), (1, 1, 0, 0), (1, 0, 0, 0),
+    ),
+    "a0": (
+        (2, 3, 0, 0), (1, 3, 0, 0),
     ),
     "a1": (
-        (2, 2, 0, 0),
+        (2, 2, 0, 0), (1, 2, 0, 0),
     ),
     "a2": (
-        (0, 2, 0, 1), (1, 1, 1, 0), (3, 1, 0, 0), (1, 1, 2, 0), (2, 2, 1, 0),
+        (0, 1, 0, 1),
     ),
     "a3": (
-        (3, 3, 0, 0), (0, 0, 0, 1), (2, 0, 1, 0),
+        (2, 0, 1, 0), (3, 1, 0, 0), (0, 0, 0, 1), (1, 1, 1, 0), (1, 1, 2, 0),
     ),
     "a4": (
-        (0, 1, 0, 1),
+        (3, 3, 0, 0),
     ),
     "xsent": (
-        (3, 0, 0, 0), (1, 1, 3, 0), (2, 0, 2, 0), (0, 1, 1, 1), (3, 0, 1, 0), (2, 0, 3, 0),
-        (2, 0, 4, 0),
+        (2, 0, 2, 0), (3, 0, 0, 0), (0, 1, 0, 2), (3, 0, 1, 0), (2, 0, 3, 0), (2, 0, 4, 0),
+        (0, 0, 0, 2),
     ),
     "zsent": (
-        (0, 0, 0, 2), (0, 1, 2, 1), (0, 1, 0, 2), (3, 0, 2, 0), (2, 2, 2, 0),
+        (0, 1, 1, 1), (0, 1, 2, 1), (1, 1, 3, 0), (0, 1, 0, 3), (3, 0, 2, 0), (2, 0, 5, 0),
+        (2, 0, 6, 0), (0, 0, 0, 3),
     ),
     "z2sent": (
-        (3, 0, 3, 0), (1, 3, 1, 0), (0, 0, 0, 3), (2, 0, 5, 0), (2, 0, 6, 0), (0, 1, 3, 1),
-        (0, 1, 1, 2), (0, 1, 2, 2), (3, 0, 4, 0), (0, 1, 0, 3),
+        (3, 0, 3, 0), (0, 1, 1, 2), (0, 1, 2, 2), (3, 0, 4, 0), (0, 1, 3, 1), (2, 0, 7, 0),
+        (0, 2, 0, 1), (3, 0, 5, 0), (1, 3, 1, 0),
     ),
     "ag1": (
-        (2, 0, 7, 0), (1, 3, 2, 0), (3, 0, 5, 0), (0, 1, 3, 2), (0, 1, 1, 3),
+        (0, 1, 1, 3), (3, 0, 6, 0), (1, 3, 2, 0), (0, 1, 2, 3), (0, 1, 3, 2),
     ),
     "ag2": (
-        (3, 0, 6, 0), (1, 3, 3, 0), (0, 1, 2, 3), (2, 2, 3, 0), (0, 2, 0, 2),
+        (3, 2, 0, 0), (1, 3, 3, 0), (2, 2, 1, 0), (0, 2, 0, 2), (2, 2, 2, 0), (3, 0, 7, 0),
+        (0, 3, 0, 1),
     ),
     "ag3": (
-        (3, 2, 0, 0), (0, 3, 0, 1), (2, 2, 4, 0),
+        (0, 3, 1, 1), (2, 2, 3, 0),
     ),
     "pr0": (
-        (3, 0, 7, 0), (0, 3, 1, 1), (0, 1, 3, 3),
+        (0, 1, 3, 3),
+    ),
+    "pr1": (
+        (2, 2, 4, 0), (0, 3, 2, 1),
     ),
     "pr2": (
-        (0, 3, 2, 1), (3, 2, 1, 0),
+        (3, 2, 1, 0), (0, 3, 3, 1),
     ),
     "pr3": (
-        (3, 2, 2, 0), (0, 3, 3, 1),
+        (3, 2, 2, 0), (2, 2, 5, 0), (0, 2, 0, 3),
     ),
     "gu": (
-        (2, 2, 5, 0), (3, 2, 3, 0), (0, 2, 0, 3), (2, 2, 6, 0), (0, 3, 0, 2), (3, 2, 4, 0),
-        (0, 3, 1, 2),
+        (0, 3, 0, 2), (2, 2, 6, 0), (0, 3, 1, 2), (3, 2, 3, 0),
     ),
     "d0": (
-        (0, 3, 2, 2), (0, 3, 3, 2), (3, 2, 5, 0), (2, 2, 7, 0),
+        (3, 2, 4, 0), (2, 2, 7, 0), (0, 3, 2, 2), (0, 3, 3, 2),
     ),
     "d1": (
-        (3, 2, 6, 0), (0, 3, 0, 3), (0, 3, 1, 3),
+        (3, 2, 5, 0), (0, 3, 0, 3), (3, 2, 6, 0), (0, 3, 1, 3),
     ),
     "d2": (
         (0, 3, 2, 3), (3, 2, 7, 0), (0, 3, 3, 3),
@@ -362,11 +368,11 @@
     resid_hbm, wo_hbm, gate_hbm, up_hbm, down_hbm,
     out_ref,
     q_ref, k_ref, v_ref, dip_ref, cri_ref, dco_ref, cro_ref, gain_ref, extra_t_ref, fng_ref,
-    wgu, wd, g_in, u_in, wo, resid,
+    wgu, wd, g_in, u_in, d_in, wo, resid,
     extra_ref, m_ref, n_ref, r_ref, o_ref, gm_ref, hm_ref,
     tot_ref, xbuf, xpre, zsrc, zbuf, s_ref, z2src, z2buf,
     mix_all, mid_ref, rows, hid_ref,
-    full_part, own_part, pair, sib_src, sib_buf, far_src, far_buf, y_src, y_buf,
+    full_part, own_part, pair, sib_src, sib_buf, far_src, far_buf, y_src, y_buf, far_out, far_in,
     local_sem, send_z, recv_z, send_x, recv_x,
     st_send, st_recv, res_send, res_recv, ag_send, ag_recv, rs_send, rs_recv,
 ):
@@ -387,7 +393,7 @@
     own = [
         pltpu.make_async_copy(src, dst, local_sem.at[i])
         for i, (src, dst) in enumerate(
-            ((gate_hbm, g_in), (up_hbm, u_in), (down_hbm, wd.at[z, x]), (resid_hbm, resid.at[block_rows(tp)]),
+            ((gate_hbm, g_in), (up_hbm, u_in), (down_hbm, d_in), (resid_hbm, resid.at[block_rows(tp)]),
              (extra_t_hbm, extra_t_ref), (k_hbm, k_ref), (q_hbm, q_ref), (v_hbm, v_ref), (dip_hbm, dip_ref),
              (cri_hbm, cri_ref), (dco_hbm, dco_ref), (cro_hbm, cro_ref), (gain_hbm, gain_ref), (fng_hbm, fng_ref), (wo_hbm, wo))
         )
@@ -395,19 +401,24 @@
     barrier = pltpu.get_barrier_semaphore()
     peers = [{"x": lax.rem(x + d, NX)} for d in range(1, NX)]
     peers += [{"z": lax.rem(z + d, NZ)} for d in range(1, NZ)]
-    peers += [{"y": lax.rem(y + d, NY)} for d in (1, NY - 1)] + [{"c": 1 - c}]
+    peers += [{"y": lax.rem(y + d, NY)} for d in range(1, NY)] + [{"c": 1 - c}]
     for peer in peers:
         pl.semaphore_signal(barrier, inc=1, device_id=peer, device_id_type=MESH)
     for copy in own:
         copy.start()
-    for copy in own[:5]:
+    for copy in own[:2]:
         copy.wait()
     hidden = g_in.shape[1]
     full = hidden // LANES * LANES
-    wgu[z, x, :, :full] = g_in[:, :full]
-    wgu[z, x, :, full : 2 * full] = u_in[:, :full]
-    tail = jnp.concatenate([g_in[:, full:].astype(F32), u_in[:, full:].astype(F32)], axis=1)
-    wgu[z, x, :, 2 * full :] = tail.astype(BF16)
+
+    def side_by_side(left, right):
+        tail = jnp.concatenate([left[:, full:].astype(F32), right[:, full:].astype(F32)], axis=1)
+        return jnp.concatenate([left[:, :full], right[:, :full], tail.astype(BF16)], axis=1)
+
+    wgu[z, x] = side_by_side(g_in[...], u_in[...])
+    own[2].wait()
+    wd[z, x] = side_by_side(d_in[: d_in.shape[0] // 2], d_in[d_in.shape[0] // 2 :])
+    own[4].wait()
     extra_t = jnp.concatenate([extra_t_ref[...], jnp.zeros((6, extra_t_ref.shape[1]), F32)], axis=0)
     pick = (iota((8, LANES), 0) == iota((8, LANES), 1) // HEAD).astype(BF16)
     extra_ref[...] = sum(dg(part, pick, 0, 0) for part in thirds(extra_t))
@@ -424,6 +435,7 @@
         part = pl.ds(0, tokens) if half is None else pl.ds(half * (tokens // 2), tokens // 2)
         return mix_all.at[part, pl.ds(pl.multiple_of(i * LANES, LANES), LANES)]
 
+    own[3].wait()
     res = Spread(resid_block, res_send, res_recv, sends)
     res.start()
 
@@ -569,6 +581,7 @@
     for i in range(width // tile):
         cols = pl.ds(i * tile, tile)
         rows[:, cols] = (mid_ref[:, cols].astype(F32) * scale * fng_ref[:, cols]).astype(BF16)
+    early = len(sends)
     mark("gu")
     g.serve("gu")
     g.whole(GQ)
@@ -582,7 +595,10 @@
 
     rest = hidden - full
     hid_ref[:, :full] = gated(both[:, :full], both[:, full : 2 * full])
-    hid_ref[:, full:] = gated(both[:, 2 * full : 2 * full + rest], both[:, 2 * full + rest :])
+    tail = gated(both[:, 2 * full : 2 * full + rest], both[:, 2 * full + rest :]).astype(F32)
+    none = jnp.zeros((tokens, LANES - rest), F32)
+    hid_ref[:, full : full + LANES] = jnp.concatenate([tail, none], axis=1).astype(BF16)
+    hid_ref[:, full + LANES :] = jnp.concatenate([none, tail], axis=1).astype(BF16)
 
     slab = width // NZ
 
@@ -606,12 +622,23 @@
             device_id={"y": lax.rem(y + (1 if up else NY - 1), NY)}, device_id_type=MESH,
         )
 
+    def straight():
+        return pltpu.make_async_remote_copy(
+            far_out, far_in, rs_send.at[last, 1], rs_recv.at[last, 1],
+            device_id={"y": lax.rem(y + 2, NY)}, device_id_type=MESH,
+        )
+
     def place(i):
         return lax.rem(z + DZ[i] + NZ, NZ)
 
     def product(n):
         for k, i in enumerate(COLS[n]):
-            full_part[n, :, k * slab : (k + 1) * slab] = dg(hid_ref[...], wd[place(i)].reshape(slab, hidden), 1, 1)
+            weights = wd[place(i)].reshape(slab // 2, 2 * hidden)
+            for side in range(2):
+                left = jnp.concatenate([hid_ref[:, :full], hid_ref[:, full + side * LANES : full + (side + 1) * LANES]], axis=1)
+                right = jnp.concatenate([weights[:, side * full : (side + 1) * full], weights[:, 2 * full :]], axis=1)
+                at = k * slab + side * (slab // 2)
+                full_part[n, :, at : at + slab // 2] = dg(left, right, 1, 1)
         for yy in range(NY):
             sib_src[n, yy, :, : wide(n)] = full_part[n, block_rows(yy * NC + 1 - c), : wide(n)].astype(BF16)
         go(to_mate(n))
@@ -624,6 +651,15 @@
             yy = lax.rem(y + d, NY)
             return full_part[n, block_rows(yy * NC + c), :w] + sib_buf[n, yy, :, :w].astype(F32)
 
+        if n == last:
+            far_out[...] = of(2).astype(BF16)
+            go(straight())
+            y_src[n, 0, :, :w] = of(1).astype(BF16)
+            go(to_y(n, 1, True))
+            y_src[n, 1, :, :w] = of(3).astype(BF16)
+            go(to_y(n, 1, False))
+            own_part[n, :, :w] = of(0)
+            return
         far = of(2).astype(BF16)
         far_src[n, 0, :, :h] = far[:, :h]
         far_src[n, 1, :, :h] = far[:, h:]
@@ -644,12 +680,34 @@
         y_src[n, 1, :, h:w] = (pair[n, 1, :, h:w] + far_buf[n, 1, :, :h].astype(F32)).astype(BF16)
         go(to_y(n, 1, False))
 
+    def in_order(packed_cols):
+        block = slab // NX // 2
+        group = iota((share, LANES), 1) // block
+        tiles = []
+        for t in range(slab // LANES):
+            out = None
+            for to in range(LANES // block):
+                at = LANES // block // 2 * t + to // 2
+                shifted = packed_cols[:, (to % 2) * (slab // 2) : (to % 2 + 1) * (slab // 2)]
+                shift = (to - at) * block % LANES
+                shifted = pltpu.roll(shifted, shift, 1) if shift else shifted
+                out = shifted if out is None else jnp.where(group == to, shifted, out)
+            tiles.append(out)
+        return jnp.concatenate(tiles, axis=1)
+
+    last = len(COLS) - 1
+
     def finish(n):
         for up in (True, False):
             to_y(n, 1, up).wait_recv()
+        if n == last:
+            straight().wait_recv()
         for k, i in enumerate(COLS[n]):
             at = slice(k * slab, (k + 1) * slab)
             acc = own_part[n, :, at] + y_buf[n, 0, :, at].astype(F32) + y_buf[n, 1, :, at].astype(F32)
+            if n == last:
+                acc += far_in[...].astype(F32)
+            acc = in_order(acc)
             cols = pl.ds(pl.multiple_of(place(i) * slab, slab), slab)
             out_ref[:, cols] = (mid_ref[block_rows(tp), cols].astype(F32) + 0.5 * acc).astype(BF16)
 
@@ -660,27 +718,27 @@
             chip_sum(n - 1)
         if n > 1:
             ring_sum(n - 2)
+        if n == last:
+            for copy in sends[:early]:
+                copy.wait_send()
         mark(f"w{n}")
         for i in COLS[n]:
             g.slab(DQ, DP, i)
         mark(f"p{n}")
         product(n)
-    last = len(COLS) - 1
+    mark("rs2")
+    ring_sum(last - 1)
     mark("cs3")
     chip_sum(last)
-    mark("rs2")
-    ring_sum(last - 1)
-    mark("fin01")
+    mark("fin0")
     for n in range(last - 1):
         finish(n)
-    mark("rs3")
-    ring_sum(last)
     mark("fin2")
     finish(last - 1)
     mark("fin3")
     finish(last)
     mark("sendwait")
-    for copy in sends:
+    for copy in sends[early:]:
         copy.wait_send()
     for d in range(1, ZG):
         pl.when(place_z + d < ZG)(lambda d=d: z_state(d).wait_send())
@@ -713,8 +771,8 @@
         out_specs=flat,
         scratch_shapes=[
             *[vm((tokens, LANES), BF16)] * 5, *[vm((1, LANES), F32)] * 3, vm((LANES // HEAD, tokens), F32), vm((1, width), F32),
-            vm((NZ, NX, shard, 2 * hidden), BF16), vm((NZ, NX, shard, hidden), BF16),
-            vm((shard, hidden), BF16), vm((shard, hidden), BF16),
+            vm((NZ, NX, shard, 2 * hidden), BF16), vm((NZ, NX, shard // 2, 2 * hidden), BF16),
+            vm((shard, hidden), BF16), vm((shard, hidden), BF16), vm((shard, hidden), BF16),
             vm(mixer_output_weight.shape, BF16), vm((tokens, width), BF16),
             vm((tokens, LANES), F32),
             vm((CHUNKS, LANES, LANES), F32), vm((CHUNKS, LANES, LANES), F32),
@@ -723,11 +781,12 @@
             vm((LANES, LANES), BF16), vm((NX - 1, LANES, LANES), BF16), vm((2 * LANES, LANES), F32),
             vm((LANES, LANES), BF16), vm((ZG - 1, LANES, LANES), BF16), vm((2 * LANES, LANES), F32),
             vm((HEAD, LANES), BF16), vm((HEAD, LANES), BF16),
-            vm((tokens, NT * LANES), BF16), vm((tokens, width), BF16), vm((tokens, width), BF16), vm((tokens, hidden), BF16),
+            vm((tokens, NT * LANES), BF16), vm((tokens, width), BF16), vm((tokens, width), BF16), vm((tokens, hidden // LANES * LANES + 2 * LANES), BF16),
             vm((parts, tokens, wide), F32), vm((parts, share, wide), F32), vm((parts, 2, share, wide), F32),
             vm((parts, NY, share, wide), BF16), vm((parts, NY, share, wide), BF16),
             vm((parts, 2, share, wide // 2), BF16), vm((parts, 2, share, wide // 2), BF16),
             vm((parts, 2, share, wide), BF16), vm((parts, 2, share, wide), BF16),
+            vm((share, len(COLS[-1]) * slab), BF16), vm((share, len(COLS[-1]) * slab), BF16),
             sem((15,)), sem((10, 8)), sem((10, 8)), sem((18, 4)), sem((18, 4)),
             sem((NX + 2 * ZG - 2,)), sem((NX + ZG - 1,)), sem((10,)), sem((10,)), sem((10,)), sem((10,)),
             sem((parts, 5)), sem((parts, 5)),

time: 75.4 us -> 74.8 us (level)
  no operation moved by 1% of the time
where the time goes in v4:
time: 74.8 us; the launch traced here: 74.7 us
  Pallas kernels  74 us (99%)
    pallas_call x1, Pallas kernels, per_device(): pl.pallas_call(kernel, name='layer', out_shape=pltpu.VMEM((share, width),...  74 us

profile of v4, /device:TPU:1, one launch (start us, length us, event | category | flops | bytes accessed | tf_op | source)
XLA Modules:
  0.0 74.7 jit_solution(15872889848192885211)
XLA Ops:
  0.0 74.0 %layer.1 = bf16[48,2048]{1,0:T(8,128)(2,1)S(1)} custom-call(bf16[384,128]{1,0:T(8,128)(2,1)} %q_hbm.1, bf16[384,128]{1,0:T(8,128)(2,1)} %k_hbm.1, bf16[384,128]{1,0:T(8,128)(2,1)} %v_hbm.1, bf16[384,128]{1,0:T(8,128)(2,1)} %dip_hbm.1, bf16[384,128]{1,0:T(8,128)(2,1)} %cri_hbm.1, f32[1,128]{1,0:T(1,128)} %bitcast.9, f32[1,128]{1,0:T(1,128)} %bitcast.10, ...), custom_call_target="tpu_custom_call" | custom-call | tf_op jit(solution)/shard_map/layer/pallas_call | solution.py:766
  74.0 0.7 copy.17

commit v5 on v4

--- a/solution.py
+++ b/solution.py
@@ -16,7 +16,7 @@
 ZG = NZ // 2
 CHUNKS = 6
 GROUP = 3
-COLS = ((0, 1, 2), (3, 4), (5, 6), (7,))
+COLS = ((0, 1, 2), (3, 4, 5), (6,), (7,))
 SP, TP, SP_TP = ("z", "x"), ("y", "c"), ("z", "x", "y", "c")
 
 
@@ -402,9 +402,11 @@
     peers = [{"x": lax.rem(x + d, NX)} for d in range(1, NX)]
     peers += [{"z": lax.rem(z + d, NZ)} for d in range(1, NZ)]
     peers += [{"y": lax.rem(y + d, NY)} for d in range(1, NY)] + [{"c": 1 - c}]
+    for copy in own[:3]:
+        copy.start()
     for peer in peers:
         pl.semaphore_signal(barrier, inc=1, device_id=peer, device_id_type=MESH)
-    for copy in own:
+    for copy in own[3:]:
         copy.start()
     for copy in own[:2]:
         copy.wait()

time: 74.8 us -> 76.9 us (1.028)
  Pallas kernels: 74 us -> 76.1 us
    pallas_call x1, Pallas kernels: 74 us -> 76.1 us  [per_device(): pl.pallas_call(kernel, name='layer', out_shape=pltpu.VMEM((share, width),...]
where the time goes in v5:
time: 76.9 us; the launch traced here: 76.8 us
  Pallas kernels  76.1 us (99%)
    pallas_call x1, Pallas kernels, per_device(): pl.pallas_call(kernel, name='layer', out_shape=pltpu.VMEM((share, width),...  76.1 us

profile of v5, /device:TPU:1, one launch (start us, length us, event | category | flops | bytes accessed | tf_op | source)
XLA Modules:
  0.0 76.8 jit_solution(16668219462049010965)
XLA Ops:
  0.0 76.1 %layer.1 = bf16[48,2048]{1,0:T(8,128)(2,1)S(1)} custom-call(bf16[384,128]{1,0:T(8,128)(2,1)} %q_hbm.1, bf16[384,128]{1,0:T(8,128)(2,1)} %k_hbm.1, bf16[384,128]{1,0:T(8,128)(2,1)} %v_hbm.1, bf16[384,128]{1,0:T(8,128)(2,1)} %dip_hbm.1, bf16[384,128]{1,0:T(8,128)(2,1)} %cri_hbm.1, f32[1,128]{1,0:T(1,128)} %bitcast.9, f32[1,128]{1,0:T(1,128)} %bitcast.10, ...), custom_call_target="tpu_custom_call" | custom-call | tf_op jit(solution)/shard_map/layer/pallas_call | solution.py:768
  76.1 0.7 copy.17
